TPU v7x, 512 devices: a whole 4x8x8 slice. The times are simulated.
512 devices in a mesh: ep: 32 (over z, x), tp: 16 (over y, core).
Axes of the slice: x: 4, y: 8, z: 8, core: 2. Of those that a mesh axis runs over, the one named last changes fastest.
Arguments:
- x_path: bfloat16 [32768, 2048], P('ep', 'tp'), may hold values from -6 to 6
- gate_path: bfloat16 [32768, 2048], P('ep', 'tp'), may hold values from -6 to 6
- conv_taps: float32 [4, 2048], P(None, 'tp'), may hold values from -3 to 3
- decay_gate_w: bfloat16 [2, 16, 128, 128], P(None, 'tp'), may hold values from -0.5 to 0.5
- input_gate_w: bfloat16 [2, 16, 128, 128], P(None, 'tp'), may hold values from -0.5 to 0.5
- decay_rate: float32 [2, 2048], P(None, 'tp'), may hold values from 0 to 1, as said below
- decay_shift: float32 [32768, 16], P('ep', 'tp'), may hold values from -1 to 0, as said below
- expert_in: bfloat16 [8192, 2048], P('ep'), may hold values from -6 to 6
- norm_gain: float32 [2048], replicated, may hold values from 0.1 to 1.9
- routes: int32 [8192, 2], P('ep'), may hold values from 0 to 31, all different within a row; in each aligned block of 16 rows (0 to 15, 16 to 31, ...) at most 2 rows name the same one
- route_scores: float32 [8192, 2], P('ep'), may hold values from 0.1 to 1
- gate_weight: bfloat16 [32, 2048, 4096], P('ep', None, 'tp'), may hold values from -0.125 to 0.125
- up_weight: bfloat16 [32, 2048, 4096], P('ep', None, 'tp'), may hold values from -0.125 to 0.125
- down_weight: bfloat16 [32, 4096, 2048], P('ep', 'tp'), may hold values from -0.09375 to 0.09375
Outputs:
- recurrent_out: bfloat16 [32768, 2048], P('ep', 'tp')
- expert_out: bfloat16 [8192, 2048], P(('ep', 'tp'))
Inputs may be any that keep to these rules, and one draw needn't show every extreme that they name: `routes`: in each aligned block of 16 rows no expert is named by more than 2 rows, and in some block some expert is named by exactly 2 rows; each row names 2 different experts. `decay_rate`: positive rates. `decay_shift`: never positive.
All inputs are finite; a program needn't handle non-finite values.
Results may differ from a plain program's by a relative error of at most 0.019.
Values may be sent and summed in bfloat16 or wider, within the bound.
A program may use at most 64 MiB of HBM per device.

v0:
```python
import jax
import jax.numpy as jnp
from jax import lax
from jax.sharding import Mesh
from jax.sharding import PartitionSpec as P

TOP_K = 2
TP = ("tp_0", "tp_1")
EP_TP = ("ep", "tp_0", "tp_1")


EPSILON = 1e-06


def with_halo(x, sides, width):
    for axis, dim in sides:
        count, length = (lax.axis_size(axis), x.shape[dim])
        up = [(i, (i + 1) % count) for i in range(count - 1)]
        down = [(j, i) for i, j in up]
        last = lax.slice_in_dim(x, length - width, length, axis=dim)
        first = lax.slice_in_dim(x, 0, width, axis=dim)
        before = lax.ppermute(last, axis, up)
        after = lax.ppermute(first, axis, down)
        x = jnp.concatenate([before, x, after], axis=dim)
    return x


def sent_to_all(x, axis):
    copies = jnp.broadcast_to(x, (lax.axis_size(axis), *x.shape))
    return lax.all_to_all(copies, axis, split_axis=0, concat_axis=0, tiled=True)


def collected_together(x, axis):
    leaves = jax.tree.leaves(x)
    turns = sorted(range(len(leaves)), key=lambda k: -leaves[k].size)
    width = (1, *leaves[turns[0]].shape)[-1]
    lines = [
        jnp.pad(leaves[k].reshape(-1), (0, -leaves[k].size % width)).reshape(-1, width)
        for k in turns
    ]
    both, at, found = (sent_to_all(jnp.concatenate(lines), axis), 0, {})
    for k, line in zip(turns, lines):
        share = both[:, at : at + len(line)].reshape(len(both), -1)
        found[k] = share[:, : leaves[k].size].reshape(-1, *leaves[k].shape)
        at += len(line)
    numbers = iter(range(len(leaves)))
    return jax.tree.map(lambda _: found[next(numbers)], x)


def joined_by_halves(pieces, combine):
    while len(jax.tree.leaves(pieces)[0]) > 1:
        pieces = jax.vmap(combine)(
            *(jax.tree.map(lambda part: part[side::2], pieces) for side in (0, 1))
        )
    return jax.tree.map(lambda part: part[0], pieces)


def entering(x, axis, combine, identity, reverse):
    count, place = (lax.axis_size(axis), lax.axis_index(axis))
    passed = jnp.arange(count) > place if reverse else jnp.arange(count) < place

    def kept(part, zero, own):
        part = jnp.where(
            passed.reshape(-1, *(1 for _ in own.shape)), part, jnp.asarray(zero, own.dtype)
        )
        return part[::-1] if reverse else part

    pieces = collected_together(x, axis)
    return joined_by_halves(jax.tree.map(kept, pieces, identity, x), combine)


def in_blocks(x, dim, count):
    shape = x.shape
    blocks = x.reshape(*shape[:dim], count, shape[dim] // count, *shape[dim + 1 :])
    return jnp.moveaxis(blocks, dim, 0)


def sum_by_chip(x, chips, core, dim):
    sizes = (lax.axis_size(chips), lax.axis_size(core))
    blocks = in_blocks(x, dim, sizes[0] * sizes[1])
    inside = blocks.shape[1:]
    blocks = blocks.reshape(*sizes, *inside).swapaxes(0, 1).reshape(-1, *inside)
    blocks = lax.psum_scatter(blocks, core, scatter_dimension=0, tiled=True)
    return lax.psum_scatter(blocks, chips, scatter_dimension=0, tiled=True)[0]


def link_pairs(earlier, later):
    return (earlier[0] * later[0], later[0] * earlier[1] + later[1])


def block_gates(conv_out, weights):
    length, channels = conv_out.shape
    heads_here = weights.shape[0]
    grouped = conv_out.reshape(length, heads_here, channels // heads_here)
    preact = jnp.einsum("thi,hij->thj", grouped, weights, preferred_element_type=jnp.float32)
    return jax.nn.sigmoid(preact).reshape(length, channels)


def local_chain(conv_out, decay_weights, input_weights, rate, shift):
    decay_gate = block_gates(conv_out, decay_weights)
    input_gate = block_gates(conv_out, input_weights)
    per_head = conv_out.shape[1] // decay_weights.shape[0]
    log_decay = -8.0 * decay_gate * rate + jnp.repeat(shift, per_head, axis=1)
    drive = jnp.sqrt(-jnp.expm1(2.0 * log_decay)) * input_gate * conv_out.astype(jnp.float32)
    return lax.associative_scan(link_pairs, (jnp.exp(log_decay), drive), axis=0)


def slot_places(routes, block_rows, capacity, experts):
    block_count = routes.shape[0] // block_rows
    flattened = routes.reshape(block_count, block_rows * routes.shape[1])
    onehot = (flattened[:, :, None] == jnp.arange(experts, dtype=jnp.int32)[None, None, :]).astype(
        jnp.int32
    )
    earlier = jnp.sum((jnp.cumsum(onehot, axis=1) - onehot) * onehot, axis=2)
    return (flattened * capacity + earlier).reshape(routes.shape)


def local(
    x_path,
    gate_path,
    conv_taps,
    decay_gate_w,
    input_gate_w,
    decay_rate,
    decay_shift,
    expert_in,
    norm_gain,
    routes,
    route_scores,
    gate_weight,
    up_weight,
    down_weight,
):
    length = x_path.shape[0]
    rimmed = with_halo(x_path, (("ep", 0),), 2)
    conv_sum = rimmed[0:length].astype(jnp.float32) * conv_taps[0]
    for offset in range(1, 4):
        conv_sum = (
            conv_sum + rimmed[offset : offset + length].astype(jnp.float32) * conv_taps[offset]
        )
    conv_out = conv_sum.astype(jnp.bfloat16)
    forward_cum, forward_local = local_chain(
        conv_out, decay_gate_w[0], input_gate_w[0], decay_rate[0], decay_shift
    )
    backward_cum, backward_local = local_chain(
        conv_out[::-1], decay_gate_w[1], input_gate_w[1], decay_rate[1], decay_shift[::-1]
    )
    neutral = (jnp.ones_like(forward_cum[-1]), jnp.zeros_like(forward_local[-1]))
    carry_forward = entering(
        (forward_cum[-1], forward_local[-1]), "ep", link_pairs, neutral, False
    )[1]
    carry_backward = entering(
        (backward_cum[-1], backward_local[-1]), "ep", link_pairs, neutral, True
    )[1]
    forward_state = forward_local + forward_cum * carry_forward[None, :]
    backward_state = (backward_local + backward_cum * carry_backward[None, :])[::-1]
    gated = jax.nn.gelu(gate_path.astype(jnp.float32))
    recurrent_out = ((forward_state + backward_state) * gated).astype(jnp.bfloat16)
    head_count = lax.axis_size(TP)
    experts = lax.axis_size("ep")
    group_rows, model = expert_in.shape
    exit_rows = group_rows // head_count
    capacity = max(2, 2 * exit_rows * TOP_K // experts)
    slots = experts * capacity
    wide_in = expert_in.astype(jnp.float32)
    scale = lax.rsqrt(jnp.mean(wide_in * wide_in, axis=1, keepdims=True) + EPSILON)
    normed = (wide_in * scale * norm_gain).astype(jnp.bfloat16)
    places = slot_places(routes, exit_rows, capacity, experts)
    slot_ids = jnp.arange(slots, dtype=jnp.int32)
    selector = jnp.sum((places[:, :, None] == slot_ids[None, None, :]).astype(jnp.bfloat16), axis=1)
    own_start = lax.axis_index(TP) * exit_rows
    own_selector = lax.dynamic_slice_in_dim(selector, own_start, exit_rows, 0)
    own_normed = lax.dynamic_slice_in_dim(normed, own_start, exit_rows, 0)
    outgoing = jnp.einsum("sp,sd->pd", own_selector, own_normed, preferred_element_type=jnp.float32)
    outgoing = outgoing.astype(jnp.bfloat16).reshape(experts, capacity, model)
    arrived = lax.all_to_all(outgoing, "ep", split_axis=0, concat_axis=0, tiled=True).reshape(
        -1, model
    )
    picked_rows = lax.all_gather(arrived, TP, axis=0, tiled=True)
    gate_pre = jnp.dot(picked_rows, gate_weight[0], preferred_element_type=jnp.float32)
    up_pre = jnp.dot(picked_rows, up_weight[0], preferred_element_type=jnp.float32)
    hidden_all = (jax.nn.silu(gate_pre) * up_pre).astype(jnp.bfloat16)
    summed = (
        sum_by_chip(
            jnp.dot(hidden_all, down_weight[0], preferred_element_type=jnp.float32).astype(
                jnp.bfloat16
            ),
            "tp_0",
            "tp_1",
            0,
        )
        .astype(jnp.float32)
        .astype(jnp.bfloat16)
    )
    returned = lax.all_to_all(
        summed.reshape(experts, capacity, model), "ep", split_axis=0, concat_axis=0, tiled=True
    ).reshape(slots, model)
    own_places = lax.dynamic_slice_in_dim(places, own_start, exit_rows, 0)
    own_scores = lax.dynamic_slice_in_dim(route_scores, own_start, exit_rows, 0)
    shares = own_scores / jnp.sum(own_scores, axis=1, keepdims=True)
    chosen = returned[own_places]
    expert_out = jnp.sum(chosen.astype(jnp.float32) * shares[:, :, None], axis=1).astype(
        jnp.bfloat16
    )
    return (recurrent_out, expert_out)


def solution(mesh):
    split = Mesh(mesh.devices.reshape(mesh.shape["ep"], 8, 2), ("ep", "tp_0", "tp_1"))
    in_specs = (
        P("ep", TP),
        P("ep", TP),
        P(None, TP),
        P(None, TP, None, None),
        P(None, TP, None, None),
        P(None, TP),
        P("ep", TP),
        P("ep", None),
        P(),
        P("ep", None),
        P("ep", None),
        P("ep", None, TP),
        P("ep", None, TP),
        P("ep", TP, None),
    )
    out_specs = (P("ep", TP), P(EP_TP, None))
    return jax.shard_map(local, mesh=split, in_specs=in_specs, out_specs=out_specs, check_vma=False)
```

profile of v0, /device:TPU:6, one launch (start us, length us, event | category | flops | bytes accessed | tf_op | source)
XLA Modules:
  0.0 247.8 jit_solution(12089783972614596150)
XLA Ops:
  7.3 1.6 multiply_reduce_fusion
  8.9 1.5 convert_element_type.69
  10.7 0.8 fusion.90
  12.4 24.4 %all_to_all.20 = bf16[32,2,2048]{2,1,0:T(2,128)(2,1)S(1)} all-to-all(bf16[32,2,2048]{2,1,0:T(2,128)(2,1)S(1)} %reshape.155), channel_id=1, replica_groups=mesh['ep'=32,'tp_0'=8,'tp_1'=2] {'ep'}, dimensions={0} | all-to-all | bytes 524288 | tf_op jit(solution)/shard_map/all_to_all | solution.py:176
  36.8 0.8 reshape.156
  37.7 0.7 fusion.75
  38.4 4.3 %collective-permute-start = (bf16[2,128]{1,0:T(2,128)(2,1)S(1)}, bf16[2,128]{1,0:T(2,128)(2,1)S(1)}, u32[]{:S(2)}, u32[]{:S(2)}) collective-permute-start(bf16[2,128]{1,0:T(2,128)(2,1)S(1)} %get-tuple-element.11), channel_id=1, source_target_pairs={{0,16},{16,32},{32,48},{48,64},{64,80},{80,96},{96,112},{112,128},... | collective-permute-start | bytes 1544 | tf_op jit(solution)/shard_map/ppermute | solution.py:22
  42.7 2.1 collective-permute-start.1
  46.5 0.7 rev.14
  47.9 2.4 collective-permute-done.1
  50.3 1.6 add_convert_fusion
  51.9 1.1 fusion.89
  53.0 1.3 fusion.16
  55.1 1.4 slice.798
  56.5 1.4 slice.802
  57.9 1.1 multiply_add_fusion.2
  60.0 0.9 multiply_add_fusion.4
  77.4 0.9 slice.868
  79.5 1.3 slice.870
  80.8 1.4 slice.797
  83.0 1.1 fusion.88
  84.1 1.3 fusion.20
  86.6 1.4 slice.922
  88.0 1.0 multiply_add_fusion.1
  105.7 0.9 slice.923
  106.5 0.9 slice.988
  108.5 1.4 slice.990
  109.8 1.3 slice.917
  112.5 0.8 fusion.83
  113.4 3.7 %fusion.25 = f32[1024,256]{1,0:T(8,128)S(1)} fusion(bf16[1024,2048]{1,0:T(8,128)(2,1)} %all-gather.2.cloned.1.call-done, bf16[1,2048,256]{2,1,0:T(8,128)(2,1)} %param.25), kind=kOutput, calls=%fused_computation.34 | convolution fusion | flops 1073741824 | bytes 6291456 | tf_op jit(solution)/shard_map/dot_general | solution.py:180
  117.2 8.9 %convolution_convert_fusion = bf16[1024,2048]{1,0:T(8,128)(2,1)} fusion(bf16[1024,2048]{1,0:T(8,128)(2,1)} %all-gather.2.cloned.1.call-done, bf16[1,256,2048]{2,1,0:T(8,128)(2,1)S(1)} %copy-done, bf16[1,2048,256]{2,1,0:T(8,128)(2,1)} %param.26, f32[1024,256]{1,0:T(8,128)S(1)} %fusion.25), kind=kOutput, calls=%fused_computation.1 | convolution fusion | flops 2151153664 | bytes 11534336 | tf_op jit(solution)/shard_map/dot_general | solution.py:185
  126.0 4.8 %copy.53 = bf16[8,2,64,2048]{3,2,0,1:T(8,128)(2,1)} copy(bf16[8,2,64,2048]{3,2,1,0:T(8,128)(2,1)} %bitcast.65) | data formatting | bytes 8388608 | tf_op jit(solution)/shard_map/reshape;reshape | solution.py:82
  133.2 1.8 fusion.42
  135.8 1.2 pad_maximum_fusion.2
  137.1 0.7 broadcast_in_dim.48
  137.8 6.2 %all-to-all-start = ((f32[32,2,128]{2,1,0:T(2,128)}), f32[32,2,128]{2,1,0:T(2,128)}, u32[]{:S(2)}, u32[]{:S(2)}) async-start(f32[32,2,128]{2,1,0:T(2,128)} %broadcast_in_dim.48), calls=%async_computation | async-start | bytes 65536 | tf_op jit(solution)/shard_map/all_to_all | solution.py:30
  152.2 0.8 fusion.56
  154.9 1.5 fusion.54
  157.0 0.9 pad.299
  157.9 1.5 pad_maximum_fusion.12
  159.4 2.2 pad.298
  162.2 1.6 add.607
  163.8 1.7 fusion.46
  166.1 0.9 pad.321
  167.1 1.7 pad.323
  168.8 0.9 pad_maximum_fusion.8
  169.8 0.9 pad.301
  170.9 1.8 fusion.41
  172.7 0.7 pad_maximum_fusion.5
  173.4 2.7 %pad.322 = f32[1024,128]{1,0:T(8,128)} pad(f32[512,128]{1,0:T(8,128)} %pad_maximum_fusion.5, f32[]{:T(128)} %constant.22.clone.1), padding=0_1_1x0_0_0 | pad | bytes 786436 | tf_op jit(solution)/shard_map/pad | solution.py:105
  176.1 1.7 pad.303
  177.7 1.0 pad_maximum_fusion.4
  178.7 1.7 pad.302
  182.4 9.8 %all-to-all-start.1 = ((f32[32,2,128]{2,1,0:T(2,128)}), f32[32,2,128]{2,1,0:T(2,128)S(1)}, u32[]{:S(2)}, u32[]{:S(2)}) async-start(f32[32,2,128]{2,1,0:T(2,128)} %broadcast_in_dim.52), calls=%async_computation.1 | async-start | bytes 65536 | tf_op jit(solution)/shard_map/all_to_all | solution.py:30
  192.2 0.9 fusion.76
  193.4 6.9 %all-to-all-done.1 = f32[32,2,128]{2,1,0:T(2,128)S(1)} async-done(((f32[32,2,128]{2,1,0:T(2,128)}), f32[32,2,128]{2,1,0:T(2,128)S(1)}, u32[]{:S(2)}, u32[]{:S(2)}) %all-to-all-start.1) | async-done | bytes 32800 | tf_op jit(solution)/shard_map/all_to_all | solution.py:30
  200.8 2.5 multiply_add_fusion
  203.3 4.7 %rev.16 = f32[1024,128]{1,0:T(8,128)} reverse(f32[1024,128]{1,0:T(8,128)} %multiply_add_fusion), dimensions={0} | reverse | bytes 1048576 | tf_op jit(solution)/shard_map/rev | solution.py:156
  208.0 8.8 %reduce-scatter.5.cloned.1.call-done = bf16[1,64,2048]{2,1,0:T(8,128)(2,1)} async-done(((bf16[8,64,2048]{2,1,0:T(8,128)(2,1)}), bf16[1,64,2048]{2,1,0:T(8,128)(2,1)}) %reduce-scatter.5.cloned.1.call-update) | async-done | bytes 262160 | tf_op jit(solution)/shard_map/reduce_scatter | solution.py:84
  216.8 1.8 reshape.158
  218.6 10.8 %all-to-all-start.3 = ((bf16[32,2,2048]{2,1,0:T(2,128)(2,1)}), bf16[32,2,2048]{2,1,0:T(2,128)(2,1)S(1)}, u32[]{:S(2)}, u32[]{:S(2)}) async-start(bf16[32,2,2048]{2,1,0:T(2,128)(2,1)} %reshape.158), calls=%async_computation.5 | async-start | bytes 524288 | tf_op jit(solution)/shard_map/all_to_all | solution.py:195
  229.5 2.1 fusion.38
  231.6 7.7 %all-to-all-done.3 = bf16[32,2,2048]{2,1,0:T(2,128)(2,1)S(1)} async-done(((bf16[32,2,2048]{2,1,0:T(2,128)(2,1)}), bf16[32,2,2048]{2,1,0:T(2,128)(2,1)S(1)}, u32[]{:S(2)}, u32[]{:S(2)}) %all-to-all-start.3) | async-done | bytes 262176 | tf_op jit(solution)/shard_map/all_to_all | solution.py:195
  240.2 1.0 multiply_reduce_fusion.1
  (497 shorter events, 61.7 us)
Async XLA Ops:
  7.2 110.0 %copy-start = (bf16[1,256,2048]{2,1,0:T(8,128)(2,1)S(1)}, bf16[1,256,2048]{2,1,0:T(8,128)(2,1)}, u32[]{:S(2)}) copy-start(bf16[1,256,2048]{2,1,0:T(8,128)(2,1)} %param.27) | copy-start | bytes 3145732
  7.2 3.2 %copy-start.31 = (s32[256,2]{0,1:T(2,128)S(1)}, s32[256,2]{0,1:T(2,128)}, u32[]{:S(2)}) copy-start(s32[256,2]{0,1:T(2,128)} %param.23) | copy-start | bytes 6148
  7.2 4.7 %copy-start.32 = (f32[2048]{0:T(1024)S(1)}, f32[2048]{0:T(1024)}, u32[]{:S(2)}) copy-start(f32[2048]{0:T(1024)} %param.22) | copy-start | bytes 24580
  7.2 37.9 %copy-start.40 = (f32[256,2]{0,1:T(2,128)S(1)}, f32[256,2]{0,1:T(2,128)}, u32[]{:S(2)}) copy-start(f32[256,2]{0,1:T(2,128)} %param.24) | copy-start | bytes 6148
  7.2 38.6 %copy-start.42 = (f32[2,128]{1,0:T(2,128)S(1)}, f32[2,128]{1,0:T(2,128)}, u32[]{:S(2)}) copy-start(f32[2,128]{1,0:T(2,128)} %param.19) | copy-start | bytes 3076
  7.2 38.6 %copy-start.41 = (f32[4,128]{1,0:T(4,128)S(1)}, f32[4,128]{1,0:T(4,128)}, u32[]{:S(2)}) copy-start(f32[4,128]{1,0:T(4,128)} %param.16) | copy-start | bytes 6148
  7.2 39.2 %copy-start.36 = (f32[1024,1]{0,1:T(1,128)S(1)}, f32[1024,1]{0,1:T(1,128)}, u32[]{:S(2)}) copy-start(f32[1024,1]{0,1:T(1,128)} %param.20) | copy-start | bytes 12292
  7.2 106.1 %all-gather.2.cloned.1.call-start = ((), (), s32[]{:S(2)}) async-start(), calls=%async_computation.6 | async-start | bytes 4456448 | tf_op jit(solution)/shard_map/all_gather | solution.py:179
  37.7 133.2 %reduce-scatter.3.cloned.1.call-start = ((), (), s32[]{:S(2)}) async-start(), calls=%async_computation.7 | async-start | bytes 6291456 | tf_op jit(solution)/shard_map/reduce_scatter | solution.py:83
  38.4 9.5 %collective-permute-start = (bf16[2,128]{1,0:T(2,128)(2,1)S(1)}, bf16[2,128]{1,0:T(2,128)(2,1)S(1)}, u32[]{:S(2)}, u32[]{:S(2)}) collective-permute-start(bf16[2,128]{1,0:T(2,128)(2,1)S(1)} %get-tuple-element.11), channel_id=1, source_target_pairs={{0,16},{16,32},{32,48},{48,64},{64,80},{80,96},{96,112},{112,128},... | collective-permute-start | bytes 1544 | tf_op jit(solution)/shard_map/ppermute | solution.py:22
  42.7 7.6 %collective-permute-start.1 = (bf16[2,128]{1,0:T(2,128)(2,1)S(1)}, bf16[2,128]{1,0:T(2,128)(2,1)S(1)}, u32[]{:S(2)}, u32[]{:S(2)}) collective-permute-start(bf16[2,128]{1,0:T(2,128)(2,1)S(1)} %get-tuple-element.10), channel_id=1, source_target_pairs={{16,0},{32,16},{48,32},{64,48},{80,64},{96,80},{112,96},{128,112},... | collective-permute-start | bytes 1544 | tf_op jit(solution)/shard_map/ppermute | solution.py:23
  54.3 28.4 %copy-start.6 = (f32[1024,128]{1,0:T(8,128)}, f32[1024,128]{1,0:T(8,128)S(1)}, u32[]{:S(2)}) copy-start(f32[1024,128]{1,0:T(8,128)S(1)} %fusion.16) | copy-start | bytes 1572868
  61.4 24.0 %copy-start.29 = (f32[4,128]{1,0:T(4,128)}, f32[4,128]{1,0:T(4,128)S(1)}, u32[]{:S(2)}) copy-start(f32[4,128]{1,0:T(4,128)S(1)} %get-tuple-element.80) | copy-start | bytes 6148
  61.4 24.0 %copy-start.30 = (f32[4,128]{1,0:T(4,128)}, f32[4,128]{1,0:T(4,128)S(1)}, u32[]{:S(2)}) copy-start(f32[4,128]{1,0:T(4,128)S(1)} %get-tuple-element.81) | copy-start | bytes 6148
  85.4 26.3 %copy-start.5 = (f32[1024,128]{1,0:T(8,128)}, f32[1024,128]{1,0:T(8,128)S(1)}, u32[]{:S(2)}) copy-start(f32[1024,128]{1,0:T(8,128)S(1)} %fusion.20) | copy-start | bytes 1572868
  89.9 27.2 %copy-start.25 = (f32[4,128]{1,0:T(4,128)}, f32[4,128]{1,0:T(4,128)S(1)}, u32[]{:S(2)}) copy-start(f32[4,128]{1,0:T(4,128)S(1)} %get-tuple-element.90) | copy-start | bytes 6148
  90.0 27.2 %copy-start.27 = (f32[4,128]{1,0:T(4,128)}, f32[4,128]{1,0:T(4,128)S(1)}, u32[]{:S(2)}) copy-start(f32[4,128]{1,0:T(4,128)S(1)} %get-tuple-element.91) | copy-start | bytes 6148
  130.9 0.8 copy-start.57
  130.9 0.8 copy-start.56
  130.9 0.9 copy-start.20
  130.9 0.9 copy-start.21
  130.9 0.9 copy-start.55
  130.9 1.0 copy-start.54
  130.9 1.0 copy-start.15
  130.9 1.0 copy-start.16
  130.9 1.0 copy-start.53
  131.0 1.1 copy-start.52
  131.0 1.2 copy-start.12
  131.0 1.2 copy-start.13
  131.0 1.2 copy-start.51
  131.0 1.2 copy-start.50
  131.0 1.3 copy-start.10
  131.0 1.3 copy-start.11
  131.0 1.4 copy-start.49
  131.0 1.4 copy-start.48
  131.0 1.5 copy-start.8
  131.1 1.6 copy-start.47
  131.5 1.4 copy-start.46
  132.3 1.0 copy-start.7
  132.7 3.1 %slice-start.1 = ((f32[1024,128]{1,0:T(8,128)}), f32[1,128]{1,0:T(1,128)S(1)}, s32[]{:S(2)}) async-start(f32[1024,128]{1,0:T(8,128)} %copy-done.6), calls=%async_computation.10 | async-start | bytes 1024 | tf_op jit(solution)/shard_map/slice | solution.py:105
  132.8 11.5 %copy-start.37 = (f32[2,128]{1,0:T(2,128)S(1)}, f32[2,128]{1,0:T(2,128)}, u32[]{:S(2)}) copy-start(f32[2,128]{1,0:T(2,128)} %slice.967) | copy-start | bytes 3076
  132.8 11.5 %copy-start.38 = (f32[2,128]{1,0:T(2,128)S(1)}, f32[2,128]{1,0:T(2,128)}, u32[]{:S(2)}) copy-start(f32[2,128]{1,0:T(2,128)} %slice.968) | copy-start | bytes 3076
  132.8 11.5 %copy-start.39 = (f32[2,128]{1,0:T(2,128)S(1)}, f32[2,128]{1,0:T(2,128)}, u32[]{:S(2)}) copy-start(f32[2,128]{1,0:T(2,128)} %slice.966) | copy-start | bytes 3076
  132.8 12.3 %copy-start.26 = (f32[4,128]{1,0:T(4,128)S(1)}, f32[4,128]{1,0:T(4,128)}, u32[]{:S(2)}) copy-start(f32[4,128]{1,0:T(4,128)} %copy-done.25) | copy-start | bytes 6148
  132.8 12.3 %copy-start.28 = (f32[4,128]{1,0:T(4,128)S(1)}, f32[4,128]{1,0:T(4,128)}, u32[]{:S(2)}) copy-start(f32[4,128]{1,0:T(4,128)} %copy-done.27) | copy-start | bytes 6148
  132.8 12.4 %copy-start.33 = (f32[3,128]{1,0:T(4,128)S(1)}, f32[3,128]{1,0:T(4,128)}, u32[]{:S(2)}) copy-start(f32[3,128]{1,0:T(4,128)} %slice.959) | copy-start | bytes 4612
  132.8 16.5 %copy-start.18 = (f32[15,128]{1,0:T(8,128)S(1)}, f32[15,128]{1,0:T(8,128)}, u32[]{:S(2)}) copy-start(f32[15,128]{1,0:T(8,128)} %slice.947) | copy-start | bytes 23044
  132.9 16.5 %copy-start.19 = (f32[15,128]{1,0:T(8,128)S(1)}, f32[15,128]{1,0:T(8,128)}, u32[]{:S(2)}) copy-start(f32[15,128]{1,0:T(8,128)} %slice.980) | copy-start | bytes 23044
  132.9 17.8 %copy-start.14 = (f32[31,128]{1,0:T(8,128)S(1)}, f32[31,128]{1,0:T(8,128)}, u32[]{:S(2)}) copy-start(f32[31,128]{1,0:T(8,128)} %slice.982) | copy-start | bytes 47620
  133.2 21.7 %copy-start.9 = (f32[127,128]{1,0:T(8,128)S(1)}, f32[127,128]{1,0:T(8,128)}, u32[]{:S(2)}) copy-start(f32[127,128]{1,0:T(8,128)} %slice.929) | copy-start | bytes 195076
  135.8 29.7 %copy-start.1 = (f32[1024,128]{1,0:T(8,128)}, f32[1024,128]{1,0:T(8,128)S(1)}, u32[]{:S(2)}) copy-start(f32[1024,128]{1,0:T(8,128)S(1)} %pad.263) | copy-start | bytes 1572868
  137.0 31.8 %copy-start.3 = (f32[1024,128]{1,0:T(8,128)}, f32[1024,128]{1,0:T(8,128)S(1)}, u32[]{:S(2)}) copy-start(f32[1024,128]{1,0:T(8,128)S(1)} %pad.262) | copy-start | bytes 1572868
  137.8 43.9 %all-to-all-start = ((f32[32,2,128]{2,1,0:T(2,128)}), f32[32,2,128]{2,1,0:T(2,128)}, u32[]{:S(2)}, u32[]{:S(2)}) async-start(f32[32,2,128]{2,1,0:T(2,128)} %broadcast_in_dim.48), calls=%async_computation | async-start | bytes 65536 | tf_op jit(solution)/shard_map/all_to_all | solution.py:30
  144.0 72.7 %reduce-scatter.5.cloned.1.call-start = ((), (), s32[]{:S(2)}) async-start(), calls=%async_computation.8 | async-start | bytes 2359296 | tf_op jit(solution)/shard_map/reduce_scatter | solution.py:84
  166.1 6.6 %copy-start.45 = (f32[1,128]{1,0:T(1,128)S(1)}, f32[1,128]{1,0:T(1,128)}, u32[]{:S(2)}) copy-start(f32[1,128]{1,0:T(1,128)} %slice.1104) | copy-start | bytes 1540
  168.8 8.9 %slice-start = ((f32[1024,128]{1,0:T(8,128)}), f32[1,128]{1,0:T(1,128)S(1)}, s32[]{:S(2)}) async-start(f32[1024,128]{1,0:T(8,128)} %copy-done.5), calls=%async_computation.9 | async-start | bytes 1024 | tf_op jit(solution)/shard_map/slice | solution.py:105
  170.7 22.3 %copy-start.44 = (pred[32]{0:T(512)(128)(4,1)S(1)}, pred[32]{0:T(512)(128)(4,1)}, u32[]{:S(2)}) copy-start(pred[32]{0:T(512)(128)(4,1)} %get-tuple-element.125) | copy-start | bytes 100
  170.8 29.6 %copy-start.43 = (pred[32]{0:T(512)(128)(4,1)S(1)}, pred[32]{0:T(512)(128)(4,1)}, u32[]{:S(2)}) copy-start(pred[32]{0:T(512)(128)(4,1)} %get-tuple-element.124) | copy-start | bytes 100
  173.4 56.1 %copy-start.2 = (f32[1024,128]{1,0:T(8,128)S(1)}, f32[1024,128]{1,0:T(8,128)}, u32[]{:S(2)}) copy-start(f32[1024,128]{1,0:T(8,128)} %copy-done.1) | copy-start | bytes 1572868
  173.4 56.1 %copy-start.4 = (f32[1024,128]{1,0:T(8,128)S(1)}, f32[1024,128]{1,0:T(8,128)}, u32[]{:S(2)}) copy-start(f32[1024,128]{1,0:T(8,128)} %copy-done.3) | copy-start | bytes 1572868
  182.4 17.9 %all-to-all-start.1 = ((f32[32,2,128]{2,1,0:T(2,128)}), f32[32,2,128]{2,1,0:T(2,128)S(1)}, u32[]{:S(2)}, u32[]{:S(2)}) async-start(f32[32,2,128]{2,1,0:T(2,128)} %broadcast_in_dim.52), calls=%async_computation.1 | async-start | bytes 65536 | tf_op jit(solution)/shard_map/all_to_all | solution.py:30
  200.8 38.6 %copy-start.17 = (s32[1024]{0:T(1024)S(1)}, s32[1024]{0:T(1024)}, u32[]{:S(2)}) copy-start(s32[1024]{0:T(1024)} %pad_clamp_fusion) | copy-start | bytes 12292
  203.3 37.0 %copy-start.22 = (f32[16,2]{1,0:T(8,128)S(1)}, f32[16,2]{1,0:T(8,128)}, u32[]{:S(2)}) copy-start(f32[16,2]{1,0:T(8,128)} %copy.55) | copy-start | bytes 388
  218.6 20.7 %all-to-all-start.3 = ((bf16[32,2,2048]{2,1,0:T(2,128)(2,1)}), bf16[32,2,2048]{2,1,0:T(2,128)(2,1)S(1)}, u32[]{:S(2)}, u32[]{:S(2)}) async-start(bf16[32,2,2048]{2,1,0:T(2,128)(2,1)} %reshape.158), calls=%async_computation.5 | async-start | bytes 524288 | tf_op jit(solution)/shard_map/all_to_all | solution.py:195
  (6 other events, 4.4 us)
Sparse Core Ops, SparseCore 0:
  37.8 41.0 all-gather.1
  131.2 17.6 reduce-scatter.2
  171.0 45.7 reduce-scatter.4
where the time goes:
time: 251 us; the launch traced here: 248 us
  local copies, waits for them, and re-layouts  84.6 us (34%)
  other arithmetic  45.6 us (18%)
  starting transfers between devices  33.6 us (13%)
  waiting for transfers between devices  25.8 us (10%)
  blocking collectives  24.4 us (10%)
  matrix products  17.6 us (7%)
  between operations  16.1 us (6%)
    slice x138, local copies, waits for them, and re-layouts, local_chain(): return lax.associative_scan(link_pairs, (jnp.exp(log_decay), drive), axis=0)  51.1 us
    all_to_all x1, blocking collectives, local(): lax.all_to_all(outgoing, 'ep', split_axis=0, concat_axis=0, tiled=True)  24.4 us
    all_to_all x2, starting transfers between devices, sent_to_all(): return lax.all_to_all(copies, axis, split_axis=0, concat_axis=0, tiled=True)  16 us
    concatenate x36, other arithmetic, local_chain(): return lax.associative_scan(link_pairs, (jnp.exp(log_decay), drive), axis=0)  13.8 us
    add x36, other arithmetic, link_pairs(): return (earlier[0] * later[0], later[0] * earlier[1] + later[1])  13.6 us
    pad x72, local copies, waits for them, and re-layouts, local_chain(): return lax.associative_scan(link_pairs, (jnp.exp(log_decay), drive), axis=0)  13.5 us
    all_to_all x1, starting transfers between devices, local(): lax.all_to_all(summed.reshape(experts, capacity, model), 'ep', split_axis...  10.8 us
    dot_general x1, matrix products, local(): jnp.dot(hidden_all, down_weight[0], preferred_element_type=jnp.float32)  8.86 us
  transfers between devices with their start and end apart: 8, of which 4 were waited for; matrix products, arithmetic and copies ran while one was open for 48% of the time, Pallas kernels for 0%

commit v1 on v0

v1 whole, which is shorter than its diff:
```python
import functools

import jax
import jax.numpy as jnp
from jax import lax
from jax.experimental import pallas as pl
from jax.experimental.pallas import tpu as pltpu
from jax.sharding import PartitionSpec as P

BF = jnp.bfloat16
F32 = jnp.float32
I32 = jnp.int32
MESH = pl.DeviceIdType.MESH
EPSILON = 1e-06
LANES = 128
EXIT = 16


def log2(n):
    return n.bit_length() - 1


def iota(shape, dim):
    return lax.broadcasted_iota(I32, shape, dim)


def shr(x, n):
    return lax.shift_right_logical(x, jnp.full(x.shape, n, I32))


def dot(a, b):
    return jnp.dot(a, b, preferred_element_type=F32)


def one_hot(mask):
    return jnp.where(mask, 1.0, 0.0).astype(BF)


def one_minus_square(log_a, a):
    z = 2.0 * log_a
    series = 1.0 + z * (1 / 2 + z * (1 / 6 + z * (1 / 24 + z * (1 / 120 + z * (1 / 720)))))
    return jnp.where(z > -0.25, -z * series, 1.0 - a * a)


def layer(
    E,
    T,
    x_hbm,
    gate_hbm,
    ein_hbm,
    wg_hbm,
    wu_hbm,
    wd_hbm,
    taps,
    dgw,
    igw,
    rate,
    shift,
    gain,
    routes,
    routes_t,
    scores,
    rec_out,
    exp_out,
    xraw,
    gatev,
    ein,
    wg,
    wu,
    wd,
    halo,
    xpad,
    sh,
    cperm,
    af,
    bf,
    ab,
    bb,
    ynat,
    seg,
    carry_send,
    carry_recv,
    dsp,
    xb,
    acc,
    perm,
    hp,
    part,
    sibp,
    rs_send,
    rs_recv,
    stk,
    ret_send,
    ret_recv,
    c_hi,
    c_lo,
    load_sem,
    halo_ss,
    halo_rs,
    carry_ss,
    carry_rs,
    dsp_ss,
    dsp_rs,
    ag_ss,
    ag_rs,
    sib_ss,
    sib_rs,
    sp_ss,
    sp_rs,
    rs_ss,
    rs_rs,
    ret_ss,
    ret_rs,
):
    NY, H = T // 2, T // 4
    S = xraw.shape[0]
    NS = S // 8
    R, D = ein.shape
    F = wg.shape[1]
    HALF = D // 2
    N = E * T
    lT, lE, lNY = log2(T), log2(E), log2(NY)

    e = lax.axis_index("ep")
    t = lax.axis_index("tp")
    y = t // 2
    c = t % 2
    sib_t = y * 2 + (1 - c)
    right_t = ((y + 1) % NY) * 2 + c
    left_t = ((y + NY - 1) % NY) * 2 + c
    ep_next = (e + 1) % E
    ep_prev = (e + E - 1) % E

    loads = [
        pltpu.make_async_copy(src, dst, load_sem.at[i])
        for i, (src, dst) in enumerate(
            ((ein_hbm, ein), (x_hbm, xraw), (wg_hbm, wg), (wu_hbm, wu), (gate_hbm, gatev), (wd_hbm, wd))
        )
    ]
    for load in loads:
        load.start()

    barrier = pltpu.get_barrier_semaphore()

    def greet(i, _):
        pl.semaphore_signal(barrier, inc=1, device_id=((e + i) % E, t), device_id_type=MESH)
        return 0

    lax.fori_loop(1, E, greet, 0)
    for peer in (sib_t, right_t, left_t):
        pl.semaphore_signal(barrier, inc=1, device_id=(e, peer), device_id_type=MESH)

    named_t = one_hot((routes_t[0:1, :] == iota((E, R), 0)) | (routes_t[1:2, :] == iota((E, R), 0)))
    rr, rc = iota((R, R), 0), iota((R, R), 1)
    earlier_t = one_hot((shr(rr, 4) == shr(rc, 4)) & (rr < rc))
    rank_t = dot(named_t, earlier_t)
    loads[0].wait()
    total = jnp.zeros((R, LANES), F32)
    for j in range(D // LANES):
        tile = ein[:, j * LANES : (j + 1) * LANES].astype(F32)
        total = total + tile * tile
    scale = lax.rsqrt(jnp.sum(total, axis=1, keepdims=True) * (1.0 / D) + EPSILON)
    own_columns = pl.ds(pl.multiple_of(t * LANES, LANES), LANES)
    normed = (ein[:, own_columns].astype(F32) * scale * gain[pl.ds(t, 1), :]).astype(BF)
    spread = one_hot(shr(iota((N, E), 0), lT) == iota((N, E), 1))
    in_block = (iota((N, R), 0) & (T - 1)) == shr(iota((N, R), 1), 4)
    for w in range(2):
        chosen = jnp.where(rank_t == float(w), named_t.astype(F32), 0.0).astype(BF)
        selector = jnp.where(in_block, dot(spread, chosen), 0.0).astype(BF)
        dsp[w] = dot(selector, normed).astype(BF)

    loads[1].wait()
    pl.semaphore_wait(barrier, E + 2)

    tail = pltpu.make_async_remote_copy(
        xraw.at[pl.ds(S - EXIT, EXIT)], halo.at[0], halo_ss.at[0], halo_rs.at[0],
        device_id=(ep_next, t), device_id_type=MESH,
    )
    head = pltpu.make_async_remote_copy(
        xraw.at[pl.ds(0, EXIT)], halo.at[1], halo_ss.at[1], halo_rs.at[1],
        device_id=(ep_prev, t), device_id_type=MESH,
    )
    tail.start()
    head.start()

    own_rows = pl.ds(pl.multiple_of(e * T, T), T)
    for w in range(2):

        def send(i, _, w=w):
            peer = (e + i) % E
            pltpu.make_async_remote_copy(
                dsp.at[w, pl.ds(pl.multiple_of(peer * T, T), T)],
                xb.at[w, y, c, own_rows],
                dsp_ss.at[w],
                dsp_rs.at[w],
                device_id=(peer, t),
                device_id_type=MESH,
            ).start()
            return 0

        lax.fori_loop(1, E, send, 0)
        xb[w, y, c, own_rows] = dsp[w, own_rows]

    n0, n1 = iota((N, N), 0), iota((N, N), 1)
    perm_block = (shr(n0, lE) & (NY - 1)) * 2 + shr(n0, lE + lNY)
    perm[...] = one_hot((shr(n1, lT) == (n0 & (E - 1))) & ((n1 & (T - 1)) == perm_block))

    own_block = pl.ds(pl.multiple_of(t * EXIT, EXIT), EXIT)
    block_routes = routes[own_block, :]
    block_scores = scores[own_block, :]
    shares = block_scores / jnp.sum(block_scores, axis=1, keepdims=True)
    ids = iota((EXIT, E), 1)
    first = block_routes[:, 0:1] == ids
    second = block_routes[:, 1:2] == ids
    below = one_hot(iota((EXIT, EXIT), 1) < iota((EXIT, EXIT), 0))
    block_rank = dot(below, one_hot(first | second))
    share_of = jnp.where(first, shares[:, 0:1], 0.0) + jnp.where(second, shares[:, 1:2], 0.0)
    rows_out = one_hot((iota((T * EXIT, EXIT), 0) & (EXIT - 1)) == iota((T * EXIT, EXIT), 1))
    columns_out = one_hot(iota((E, N), 0) == shr(iota((E, N), 1), lT))
    same_tile = shr(iota((T * EXIT, N), 0), 4) == (iota((T * EXIT, N), 1) & (T - 1))
    for w in range(2):
        weight = jnp.where(block_rank == float(w), share_of, 0.0)
        high = weight.astype(BF)
        low = (weight - high.astype(F32)).astype(BF)
        for piece, table in ((high, c_hi), (low, c_lo)):
            wide = dot(dot(rows_out, piece).astype(BF), columns_out)
            table[w] = jnp.where(same_tile, wide, 0.0).astype(BF)

    xpad[pl.ds(EXIT, S), :] = xraw[...].astype(F32)
    for s in range(NS):
        sh[pl.ds(s * 8, 8), :] = jnp.broadcast_to(shift[:, s : s + 1], (8, LANES))
    tail.wait_recv()
    head.wait_recv()
    xpad[pl.ds(0, EXIT), :] = jnp.where(e > 0, halo[0].astype(F32), 0.0)
    xpad[pl.ds(EXIT + S, EXIT), :] = jnp.where(e < E - 1, halo[1].astype(F32), 0.0)

    def strided(s):
        return xpad[pl.ds(EXIT + s, 8, stride=NS), :]

    tap = [taps[k : k + 1, :] for k in range(4)]

    def conv(s, held):
        v0, v1, v2 = held
        v3 = strided(s + 1)
        value = v0 * tap[0] + v1 * tap[1] + v2 * tap[2] + v3 * tap[3]
        cperm[pl.ds(pl.multiple_of(s * 8, 8), 8), :] = value.astype(BF).astype(F32)
        return v1, v2, v3

    lax.fori_loop(0, NS, conv, (strided(-2), strided(-1), strided(0)), unroll=8)

    CH = min(128, S)

    def gates(i, _):
        rows = pl.ds(pl.multiple_of(i * CH, CH), CH)
        value = cperm[rows, :]
        value_b = value.astype(BF)
        shift_here = sh[rows, :]
        for d, (a_ref, b_ref) in enumerate(((af, bf), (ab, bb))):
            decay_gate = jax.nn.sigmoid(dot(value_b, dgw[d, 0]))
            input_gate = jax.nn.sigmoid(dot(value_b, igw[d, 0]))
            log_decay = -8.0 * decay_gate * rate[d : d + 1, :] + shift_here
            decay = jnp.exp(log_decay)
            rest = one_minus_square(log_decay, decay)
            root = rest * lax.rsqrt(jnp.maximum(rest, 1e-37))
            a_ref[rows, :] = decay
            b_ref[rows, :] = root * input_gate * value
        return 0

    lax.fori_loop(0, S // CH, gates, 0)

    def at(s):
        return pl.ds(pl.multiple_of(s * 8, 8), 8)

    def summing(s, held):
        hf, pf, hb, pb = held
        a, b = af[at(s), :], bf[at(s), :]
        a2, b2 = ab[at(NS - 1 - s), :], bb[at(NS - 1 - s), :]
        return a * hf + b, a * pf, a2 * hb + b2, a2 * pb

    zero, one = jnp.zeros((8, LANES), F32), jnp.ones((8, LANES), F32)
    hf, pf, hb, pb = lax.fori_loop(0, NS, summing, (zero, one, zero, one), unroll=8)
    for k, value in enumerate((pf, hf, pb, hb)):
        seg[k] = value

    def segment(k, g):
        return seg[k, g : g + 1, :]

    ones = jnp.ones((1, LANES), F32)
    fa, fb, ba, bb_ = ones, ones * 0.0, ones, ones * 0.0
    for g in range(8):
        fa, fb = segment(0, g) * fa, segment(0, g) * fb + segment(1, g)
        ba, bb_ = segment(2, 7 - g) * ba, segment(2, 7 - g) * bb_ + segment(3, 7 - g)
    summary = jnp.concatenate([fa, fb, ba, bb_, jnp.zeros((4, LANES), F32)], axis=0)
    carry_send[...] = summary
    carry_recv[e] = summary

    def send_carry(i, _):
        pltpu.make_async_remote_copy(
            carry_send, carry_recv.at[e], carry_ss, carry_rs,
            device_id=((e + i) % E, t), device_id_type=MESH,
        ).start()
        return 0

    lax.fori_loop(1, E, send_carry, 0)

    def gather_copy(w, direction, hop, rows):
        source = (y + NY - hop) % NY if direction == 0 else (y + hop) % NY
        block = xb.at[w, source, c, rows]
        return pltpu.make_async_remote_copy(
            block, block, ag_ss.at[w, direction, hop], ag_rs.at[w, direction, hop],
            device_id=(e, right_t if direction == 0 else left_t), device_id_type=MESH,
        )

    def arrived_gather(w, direction, hop, rows):
        source = (y + 2 * NY - hop - 1) % NY if direction == 0 else (y + hop + 1) % NY
        block = xb.at[w, source, c, rows]
        pltpu.make_async_copy(block, block, ag_rs.at[w, direction, hop]).wait()

    whole = pl.ds(0, N)
    halves = (pl.ds(0, N // 2), pl.ds(N // 2, N // 2))

    def forward(w, direction, hop):
        if isinstance(hop, int):
            gather_copy(w, direction, hop, halves[direction] if hop == H - 1 else whole).start()

    def sibling_copy(w, source, index):
        block = xb.at[w, source, c]
        return pltpu.make_async_remote_copy(
            block, block, sib_ss.at[w, index], sib_rs.at[w, index],
            device_id=(e, sib_t), device_id_type=MESH,
        )

    def sibling_arrived(w, source, index):
        block = xb.at[w, source, 1 - c]
        pltpu.make_async_copy(block, block, sib_rs.at[w, index]).wait()

    def multiply(w, source, fresh):
        rows = jnp.concatenate([xb[w, source, 0], xb[w, source, 1]], axis=1)
        depth = pl.ds(pl.multiple_of(source * 2 * LANES, 2 * LANES), 2 * LANES)
        for k, weight in enumerate((wg, wu)):
            product = dot(rows, weight[depth, :])
            if fresh:
                acc[w, k] = product
            else:
                acc[w, k] += product

    arrivals = pl.ds(0, (E - 1) * T)
    for w in range(2):
        block = xb.at[w, y, c, arrivals]
        pltpu.make_async_copy(block, block, dsp_rs.at[w]).wait()
        forward(w, 0, 0)
        forward(w, 1, 0)
        sibling_copy(w, y, 0).start()

    pltpu.make_async_copy(
        carry_recv.at[pl.ds(0, E - 1)], carry_recv.at[pl.ds(0, E - 1)], carry_rs
    ).wait()

    def fold(i, held):
        f, b = held
        one_way = carry_recv[i]
        j = E - 1 - i
        other = carry_recv[j]
        f = jnp.where(i < e, one_way[0:1] * f + one_way[1:2], f)
        b = jnp.where(j > e, other[2:3] * b + other[3:4], b)
        return f, b

    f, b = lax.fori_loop(0, E, fold, (ones * 0.0, ones * 0.0))
    f_rows, b_rows = [f], [b]
    for g in range(7):
        f_rows.append(segment(0, g) * f_rows[-1] + segment(1, g))
        b_rows.insert(0, segment(2, 7 - g) * b_rows[0] + segment(3, 7 - g))
    f_in, b_in = jnp.concatenate(f_rows, axis=0), jnp.concatenate(b_rows, axis=0)

    def states(s, held):
        hf, hb = held
        r = NS - 1 - s
        hf = af[at(s), :] * hf + bf[at(s), :]
        hb = ab[at(r), :] * hb + bb[at(r), :]
        bf[at(s), :] = hf
        bb[at(r), :] = hb
        return hf, hb

    lax.fori_loop(0, NS, states, (f_in, b_in), unroll=8)

    def natural(s, _):
        ynat[pl.ds(s, 8, stride=NS), :] = bf[at(s), :] + bb[at(s), :]
        return 0

    lax.fori_loop(0, NS, natural, 0, unroll=8)
    loads[4].wait()

    def finish(i, _):
        rows = pl.ds(pl.multiple_of(i * CH, CH), CH)
        rec_out[rows, :] = (ynat[rows, :] * jax.nn.gelu(gatev[rows, :].astype(F32))).astype(BF)
        return 0

    lax.fori_loop(0, S // CH, finish, 0)

    loads[2].wait()
    loads[3].wait()
    for w in range(2):
        sibling_arrived(w, y, 0)
        multiply(w, y, True)

    for hop in range(1, H):
        rights, lefts = (y + NY - hop) % NY, (y + hop) % NY
        for w in range(2):
            arrived_gather(w, 0, hop - 1, whole)
            forward(w, 0, hop)
            arrived_gather(w, 1, hop - 1, whole)
            forward(w, 1, hop)
            sibling_copy(w, rights, 2 * hop - 1).start()
            sibling_copy(w, lefts, 2 * hop).start()
        for w in range(2):
            sibling_arrived(w, rights, 2 * hop - 1)
            multiply(w, rights, False)
            sibling_arrived(w, lefts, 2 * hop)
            multiply(w, lefts, False)

    far = (y + H) % NY
    for w in range(2):
        arrived_gather(w, 0, H - 1, halves[0])
        arrived_gather(w, 1, H - 1, halves[1])
        sibling_copy(w, far, NY - 1).start()

    def reduce_copy(w, direction, step):
        return pltpu.make_async_remote_copy(
            rs_send.at[w, direction, step], rs_recv.at[w, direction, step],
            rs_ss.at[w, direction, step], rs_rs.at[w, direction, step],
            device_id=(e, right_t if direction == 0 else left_t), device_id_type=MESH,
        )

    def pair_copy(w, direction):
        return pltpu.make_async_remote_copy(
            part.at[w, direction, 1 - c], sibp.at[w, direction],
            sp_ss.at[w, direction], sp_rs.at[w, direction],
            device_id=(e, sib_t), device_id_type=MESH,
        )

    def pair_sum(w, direction, to):
        return part[w, direction, c, to].astype(F32) + sibp[w, direction, to].astype(F32)

    loads[5].wait()
    TILE = min(256, HALF)
    for w in range(2):
        sibling_arrived(w, far, NY - 1)
        multiply(w, far, False)
        hidden = (jax.nn.silu(acc[w, 0]) * acc[w, 1]).astype(BF)
        hp[...] = dot(perm[...], hidden).astype(BF)
        for direction in range(2):

            def down(n, _, w=w, direction=direction):
                here = pl.ds(pl.multiple_of(n * TILE, TILE), TILE)
                there = pl.ds(pl.multiple_of(direction * HALF + n * TILE, TILE), TILE)
                product = dot(hp[...], wd[:, there]).astype(BF)
                part[w, direction, :, :, :, here] = product.reshape(2, NY, E, TILE)
                return 0

            lax.fori_loop(0, HALF // TILE, down, 0)
            pair_copy(w, direction).start()
        for direction in range(2):
            pair_copy(w, direction).wait_recv()
            to = (y + NY - 1) % NY if direction == 0 else (y + 1) % NY
            rs_send[w, direction, 0] = pair_sum(w, direction, to).astype(BF)
            reduce_copy(w, direction, 0).start()

    def ring(step, _):
        for w in range(2):
            for direction in range(2):
                to = (y + 2 * NY - 1 - step) % NY if direction == 0 else (y + 1 + step) % NY
                base = pair_sum(w, direction, to)
                reduce_copy(w, direction, step - 1).wait_recv()
                value = base + rs_recv[w, direction, step - 1].astype(F32)
                rs_send[w, direction, step] = value.astype(BF)
                reduce_copy(w, direction, step).start()
        return 0

    lax.fori_loop(1, NY - 1, ring, 0)

    for w in range(2):
        for direction in range(2):
            base = pair_sum(w, direction, y)
            reduce_copy(w, direction, NY - 2).wait_recv()
            value = base + rs_recv[w, direction, NY - 2].astype(F32)
            for j in range(HALF // LANES):
                place = direction * (HALF // LANES) + j
                stk[pl.ds(place, E, stride=T), :] = value[:, j * LANES : (j + 1) * LANES]
        ret_send[w] = stk[...].astype(BF)

        def send_back(i, _, w=w):
            peer = (e + i) % E
            pltpu.make_async_remote_copy(
                ret_send.at[w, pl.ds(pl.multiple_of(peer * T, T), T)],
                ret_recv.at[w, own_rows],
                ret_ss.at[w],
                ret_rs.at[w],
                device_id=(peer, t),
                device_id_type=MESH,
            ).start()
            return 0

        lax.fori_loop(1, E, send_back, 0)
        ret_recv[w, own_rows] = ret_send[w, own_rows]

    out = jnp.zeros((T * EXIT, LANES), F32)
    for w in range(2):
        block = ret_recv.at[w, arrivals]
        pltpu.make_async_copy(block, block, ret_rs.at[w]).wait()
        out = out + dot(c_hi[w], ret_recv[w]) + dot(c_lo[w], ret_recv[w])
    for j in range(T):
        exp_out[:, j * LANES : (j + 1) * LANES] = out[j * EXIT : (j + 1) * EXIT, :].astype(BF)

    tail.wait_send()
    head.wait_send()
    sent = carry_recv.at[pl.ds(0, E - 1)]
    pltpu.make_async_copy(sent, sent, carry_ss).wait()
    for w in range(2):
        for ref, sem in ((dsp, dsp_ss), (ret_send, ret_ss)):
            block = ref.at[w, arrivals]
            pltpu.make_async_copy(block, block, sem.at[w]).wait()
        for hop in range(H):
            for direction in range(2):
                gather_copy(w, direction, hop, halves[direction] if hop == H - 1 else whole).wait_send()
        for index in range(NY):
            sibling_copy(w, y, index).wait_send()
        for direction in range(2):
            pair_copy(w, direction).wait_send()
            for step in range(NY - 1):
                reduce_copy(w, direction, step).wait_send()


def local(
    E, T, x_path, gate_path, conv_taps, decay_gate_w, input_gate_w, decay_rate, decay_shift,
    expert_in, norm_gain, routes, route_scores, gate_weight, up_weight, down_weight,
):
    S = x_path.shape[0]
    R, D = expert_in.shape
    F = gate_weight.shape[2]
    NY, H, N, HALF = T // 2, T // 4, E * T, D // 2
    anywhere = pl.BlockSpec(memory_space=pl.ANY)
    vmem = pl.BlockSpec(memory_space=pltpu.VMEM)
    dma = pltpu.SemaphoreType.DMA
    rows = pltpu.VMEM((S, LANES), F32)
    scratch = [
        pltpu.VMEM((S, LANES), BF),
        pltpu.VMEM((S, LANES), BF),
        pltpu.VMEM((R, D), BF),
        pltpu.VMEM((D, F), BF),
        pltpu.VMEM((D, F), BF),
        pltpu.VMEM((F, D), BF),
        pltpu.VMEM((2, EXIT, LANES), BF),
        pltpu.VMEM((S + 2 * EXIT, LANES), F32),
        rows,
        rows,
        rows,
        rows,
        rows,
        rows,
        rows,
        pltpu.VMEM((4, 8, LANES), F32),
        pltpu.VMEM((8, LANES), F32),
        pltpu.VMEM((E, 8, LANES), F32),
        pltpu.VMEM((2, N, LANES), BF),
        pltpu.VMEM((2, NY, 2, N, LANES), BF),
        pltpu.VMEM((2, 2, N, F), F32),
        pltpu.VMEM((N, N), BF),
        pltpu.VMEM((N, F), BF),
        pltpu.VMEM((2, 2, 2, NY, E, HALF), BF),
        pltpu.VMEM((2, 2, NY, E, HALF), BF),
        pltpu.VMEM((2, 2, NY - 1, E, HALF), BF),
        pltpu.VMEM((2, 2, NY - 1, E, HALF), BF),
        pltpu.VMEM((N, LANES), F32),
        pltpu.VMEM((2, N, LANES), BF),
        pltpu.VMEM((2, N, LANES), BF),
        pltpu.VMEM((2, T * EXIT, N), BF),
        pltpu.VMEM((2, T * EXIT, N), BF),
        dma((6,)),
        dma((2,)),
        dma((2,)),
        dma,
        dma,
        dma((2,)),
        dma((2,)),
        dma((2, 2, H)),
        dma((2, 2, H)),
        dma((2, NY)),
        dma((2, NY)),
        dma((2, 2)),
        dma((2, 2)),
        dma((2, 2, NY - 1)),
        dma((2, 2, NY - 1)),
        dma((2,)),
        dma((2,)),
    ]
    return pl.pallas_call(
        functools.partial(layer, E, T),
        out_shape=(
            jax.ShapeDtypeStruct((S, LANES), BF),
            jax.ShapeDtypeStruct((EXIT, D), BF),
        ),
        in_specs=[anywhere] * 6 + [vmem] * 9,
        out_specs=(vmem, vmem),
        scratch_shapes=scratch,
        compiler_params=pltpu.CompilerParams(
            collective_id=0, has_side_effects=True, vmem_limit_bytes=60 * 1024 * 1024
        ),
        name="layer",
    )(
        x_path,
        gate_path,
        expert_in,
        gate_weight.reshape(D, F),
        up_weight.reshape(D, F),
        down_weight.reshape(F, D),
        conv_taps,
        decay_gate_w,
        input_gate_w,
        decay_rate,
        decay_shift.reshape(8, S // 8),
        norm_gain.reshape(D // LANES, LANES),
        routes,
        routes.T,
        route_scores,
    )


def solution(mesh):
    in_specs = (
        P("ep", "tp"),
        P("ep", "tp"),
        P(None, "tp"),
        P(None, "tp", None, None),
        P(None, "tp", None, None),
        P(None, "tp"),
        P("ep", "tp"),
        P("ep", None),
        P(),
        P("ep", None),
        P("ep", None),
        P("ep", None, "tp"),
        P("ep", None, "tp"),
        P("ep", "tp", None),
    )
    out_specs = (P("ep", "tp"), P(("ep", "tp"), None))
    step = functools.partial(local, mesh.shape["ep"], mesh.shape["tp"])
    return jax.shard_map(step, mesh=mesh, in_specs=in_specs, out_specs=out_specs, check_vma=False)
```

time: 251 us -> 97.2 us (0.39); the launches traced: 248 us -> 97.1 us
  Pallas kernels: 0 us -> 91.8 us
  local copies, waits for them, and re-layouts: 84.6 us -> 4.61 us
  other arithmetic: 45.6 us -> 0 us
  starting transfers between devices: 33.6 us -> 0 us
  waiting for transfers between devices: 25.8 us -> 0 us
  blocking collectives: 24.4 us -> 0 us
  matrix products: 17.6 us -> 0 us
  between operations: 16.1 us -> 0.66 us
    pallas_call x0 -> x1, Pallas kernels: none -> 91.8 us  [local(): pl.pallas_call(functools.partial(layer, E, T), out_shape=(jax.ShapeDtypeS...]
    slice x177 -> x0, local copies, waits for them, and re-layouts: 53.2 us -> none  [the longest x138 51.1 us: local_chain(): return lax.associative_scan(link_pairs, (jnp.exp(log_decay), drive), axis=0)]
    all_to_all x3 -> x0, starting transfers between devices: 26.9 us -> none  [the longest x2 16 us: sent_to_all(): return lax.all_to_all(copies, axis, split_axis=0, concat_axis=0, tiled=True)]
    all_to_all x1 -> x0, blocking collectives: 24.4 us -> none  [local(): lax.all_to_all(outgoing, 'ep', split_axis=0, concat_axis=0, tiled=True)]
    add x76 -> x0, other arithmetic: 20.7 us -> none  [the longest x36 13.6 us: link_pairs(): return (earlier[0] * later[0], later[0] * earlier[1] + later[1])]
    dot_general x7 -> x0, matrix products: 17.6 us -> none  [the longest x1 8.86 us: local(): jnp.dot(hidden_all, down_weight[0], preferred_element_type=jnp.float32)]
    all_to_all x3 -> x0, waiting for transfers between devices: 14.6 us -> none  [the longest x1 7.68 us: local(): lax.all_to_all(summed.reshape(experts, capacity, model), 'ep', split_axis...]
    concatenate x38 -> x0, other arithmetic: 13.9 us -> none  [the longest x36 13.8 us: local_chain(): return lax.associative_scan(link_pairs, (jnp.exp(log_decay), drive), axis=0)]
  transfers between devices with their start and end apart: 8 -> 0, of which waited for: 4 -> 0; matrix products, arithmetic and copies ran while one was open for 48% -> 0% of each run, Pallas kernels for 0% -> 0%
where the time goes in v1:
time: 97.2 us; the launch traced here: 97.1 us
  Pallas kernels  91.8 us (94%)
  local copies, waits for them, and re-layouts  4.61 us (5%)
    pallas_call x1, Pallas kernels, local(): pl.pallas_call(functools.partial(layer, E, T), out_shape=(jax.ShapeDtypeS...  91.8 us
    unnamed x10, local copies, waits for them, and re-layouts  4.61 us

profile of v1, /device:TPU:6, one launch (start us, length us, event | category | flops | bytes accessed | tf_op | source)
XLA Modules:
  0.0 97.1 jit_solution(3491140913609026614)
XLA Ops:
  0.6 0.0 copy-start.2
  0.6 0.7 copy-done.2
  1.3 0.0 copy-start.1
  1.3 0.8 copy.17.scores
  2.1 0.0 copy-done.1
  2.1 0.8 copy.16.routes
  2.9 91.8 %layer.1 = (bf16[1024,128]{1,0:T(8,128)(2,1)}, bf16[16,2048]{1,0:T(8,128)(2,1)}) custom-call(bf16[1024,128]{1,0:T(8,128)(2,1)} %x_hbm.1, bf16[1024,128]{1,0:T(8,128)(2,1)} %gate_hbm.1, bf16[256,2048]{1,0:T(8,128)(2,1)} %ein_hbm.1, bf16[2048,256]{1,0:T(8,128)(2,1)} %bitcast.6, bf16[2048,256]{1,0:T(8,128)(2,1)} %bitcast.7, bf16[256,2048]{1,0:T(8,128)(2,1)} %bitcast.8, ...), custom_call_target="tpu_custom_call" | custom-call | tf_op jit(solution)/shard_map/layer/pallas_call | solution.py:596
  94.7 0.0 copy-start
  94.7 1.7 %copy.20 = bf16[1024,128]{1,0:T(8,128)(2,1)} copy(bf16[1024,128]{1,0:T(8,128)(2,1)} %get-tuple-element.4) | data formatting | bytes 524288
  96.4 0.0 copy-done
  96.4 0.6 copy.21
Async XLA Ops:
  0.6 0.7 copy-start.2
  1.3 0.8 copy-start.1
  94.7 1.7 %copy-start = (bf16[16,2048]{1,0:T(8,128)(2,1)S(1)}, bf16[16,2048]{1,0:T(8,128)(2,1)}, u32[]{:S(2)}) copy-start(bf16[16,2048]{1,0:T(8,128)(2,1)} %get-tuple-element.5) | copy-start | bytes 196612

commit v2 on v1

--- a/solution.py
+++ b/solution.py
@@ -57,9 +57,8 @@
     rate,
     shift,
     gain,
-    routes,
     routes_t,
-    scores,
+    scores_t,
     rec_out,
     exp_out,
     xraw,
@@ -150,7 +149,10 @@
     for peer in (sib_t, right_t, left_t):
         pl.semaphore_signal(barrier, inc=1, device_id=(e, peer), device_id_type=MESH)
 
-    named_t = one_hot((routes_t[0:1, :] == iota((E, R), 0)) | (routes_t[1:2, :] == iota((E, R), 0)))
+    ids = iota((E, R), 0)
+    first_t = routes_t[0:1, :] == ids
+    second_t = routes_t[1:2, :] == ids
+    named_t = one_hot(first_t | second_t)
     rr, rc = iota((R, R), 0), iota((R, R), 1)
     earlier_t = one_hot((shr(rr, 4) == shr(rc, 4)) & (rr < rc))
     rank_t = dot(named_t, earlier_t)
@@ -205,25 +207,19 @@
     perm_block = (shr(n0, lE) & (NY - 1)) * 2 + shr(n0, lE + lNY)
     perm[...] = one_hot((shr(n1, lT) == (n0 & (E - 1))) & ((n1 & (T - 1)) == perm_block))
 
-    own_block = pl.ds(pl.multiple_of(t * EXIT, EXIT), EXIT)
-    block_routes = routes[own_block, :]
-    block_scores = scores[own_block, :]
-    shares = block_scores / jnp.sum(block_scores, axis=1, keepdims=True)
-    ids = iota((EXIT, E), 1)
-    first = block_routes[:, 0:1] == ids
-    second = block_routes[:, 1:2] == ids
-    below = one_hot(iota((EXIT, EXIT), 1) < iota((EXIT, EXIT), 0))
-    block_rank = dot(below, one_hot(first | second))
-    share_of = jnp.where(first, shares[:, 0:1], 0.0) + jnp.where(second, shares[:, 1:2], 0.0)
-    rows_out = one_hot((iota((T * EXIT, EXIT), 0) & (EXIT - 1)) == iota((T * EXIT, EXIT), 1))
+    shares_t = scores_t[...] / (scores_t[0:1, :] + scores_t[1:2, :])
+    share_of = jnp.where(first_t, shares_t[0:1, :], 0.0) + jnp.where(second_t, shares_t[1:2, :], 0.0)
+    own_row = t * EXIT + (iota((T * EXIT, R), 0) & (EXIT - 1))
+    rows_out = one_hot(own_row == iota((T * EXIT, R), 1))
     columns_out = one_hot(iota((E, N), 0) == shr(iota((E, N), 1), lT))
     same_tile = shr(iota((T * EXIT, N), 0), 4) == (iota((T * EXIT, N), 1) & (T - 1))
     for w in range(2):
-        weight = jnp.where(block_rank == float(w), share_of, 0.0)
+        weight = jnp.where(rank_t == float(w), share_of, 0.0)
         high = weight.astype(BF)
         low = (weight - high.astype(F32)).astype(BF)
         for piece, table in ((high, c_hi), (low, c_lo)):
-            wide = dot(dot(rows_out, piece).astype(BF), columns_out)
+            picked = lax.dot_general(rows_out, piece, (((1,), (1,)), ((), ())), preferred_element_type=F32)
+            wide = dot(picked.astype(BF), columns_out)
             table[w] = jnp.where(same_tile, wide, 0.0).astype(BF)
 
     xpad[pl.ds(EXIT, S), :] = xraw[...].astype(F32)
@@ -290,14 +286,17 @@
     for g in range(8):
         fa, fb = segment(0, g) * fa, segment(0, g) * fb + segment(1, g)
         ba, bb_ = segment(2, 7 - g) * ba, segment(2, 7 - g) * bb_ + segment(3, 7 - g)
-    summary = jnp.concatenate([fa, fb, ba, bb_, jnp.zeros((4, LANES), F32)], axis=0)
-    carry_send[...] = summary
-    carry_recv[e] = summary
+    ahead = jnp.concatenate([fa, fb], axis=0)
+    behind = jnp.concatenate([ba, bb_], axis=0)
+    carry_send[0] = ahead
+    carry_send[1] = behind
+    carry_recv[e] = ahead
 
     def send_carry(i, _):
+        peer = (e + i) % E
         pltpu.make_async_remote_copy(
-            carry_send, carry_recv.at[e], carry_ss, carry_rs,
-            device_id=((e + i) % E, t), device_id_type=MESH,
+            carry_send.at[(peer < e).astype(I32)], carry_recv.at[e], carry_ss, carry_rs,
+            device_id=(peer, t), device_id_type=MESH,
         ).start()
         return 0
 
@@ -351,51 +350,6 @@
         forward(w, 0, 0)
         forward(w, 1, 0)
         sibling_copy(w, y, 0).start()
-
-    pltpu.make_async_copy(
-        carry_recv.at[pl.ds(0, E - 1)], carry_recv.at[pl.ds(0, E - 1)], carry_rs
-    ).wait()
-
-    def fold(i, held):
-        f, b = held
-        one_way = carry_recv[i]
-        j = E - 1 - i
-        other = carry_recv[j]
-        f = jnp.where(i < e, one_way[0:1] * f + one_way[1:2], f)
-        b = jnp.where(j > e, other[2:3] * b + other[3:4], b)
-        return f, b
-
-    f, b = lax.fori_loop(0, E, fold, (ones * 0.0, ones * 0.0))
-    f_rows, b_rows = [f], [b]
-    for g in range(7):
-        f_rows.append(segment(0, g) * f_rows[-1] + segment(1, g))
-        b_rows.insert(0, segment(2, 7 - g) * b_rows[0] + segment(3, 7 - g))
-    f_in, b_in = jnp.concatenate(f_rows, axis=0), jnp.concatenate(b_rows, axis=0)
-
-    def states(s, held):
-        hf, hb = held
-        r = NS - 1 - s
-        hf = af[at(s), :] * hf + bf[at(s), :]
-        hb = ab[at(r), :] * hb + bb[at(r), :]
-        bf[at(s), :] = hf
-        bb[at(r), :] = hb
-        return hf, hb
-
-    lax.fori_loop(0, NS, states, (f_in, b_in), unroll=8)
-
-    def natural(s, _):
-        ynat[pl.ds(s, 8, stride=NS), :] = bf[at(s), :] + bb[at(s), :]
-        return 0
-
-    lax.fori_loop(0, NS, natural, 0, unroll=8)
-    loads[4].wait()
-
-    def finish(i, _):
-        rows = pl.ds(pl.multiple_of(i * CH, CH), CH)
-        rec_out[rows, :] = (ynat[rows, :] * jax.nn.gelu(gatev[rows, :].astype(F32))).astype(BF)
-        return 0
-
-    lax.fori_loop(0, S // CH, finish, 0)
 
     loads[2].wait()
     loads[3].wait()
@@ -419,10 +373,6 @@
             multiply(w, lefts, False)
 
     far = (y + H) % NY
-    for w in range(2):
-        arrived_gather(w, 0, H - 1, halves[0])
-        arrived_gather(w, 1, H - 1, halves[1])
-        sibling_copy(w, far, NY - 1).start()
 
     def reduce_copy(w, direction, step):
         return pltpu.make_async_remote_copy(
@@ -444,6 +394,9 @@
     loads[5].wait()
     TILE = min(256, HALF)
     for w in range(2):
+        arrived_gather(w, 0, H - 1, halves[0])
+        arrived_gather(w, 1, H - 1, halves[1])
+        sibling_copy(w, far, NY - 1).start()
         sibling_arrived(w, far, NY - 1)
         multiply(w, far, False)
         hidden = (jax.nn.silu(acc[w, 0]) * acc[w, 1]).astype(BF)
@@ -502,6 +455,51 @@
 
         lax.fori_loop(1, E, send_back, 0)
         ret_recv[w, own_rows] = ret_send[w, own_rows]
+
+    pltpu.make_async_copy(
+        carry_recv.at[pl.ds(0, E - 1)], carry_recv.at[pl.ds(0, E - 1)], carry_rs
+    ).wait()
+
+    def fold(i, held):
+        f, b = held
+        one_way = carry_recv[i]
+        j = E - 1 - i
+        other = carry_recv[j]
+        f = jnp.where(i < e, one_way[0:1] * f + one_way[1:2], f)
+        b = jnp.where(j > e, other[0:1] * b + other[1:2], b)
+        return f, b
+
+    f, b = lax.fori_loop(0, E, fold, (ones * 0.0, ones * 0.0))
+    f_rows, b_rows = [f], [b]
+    for g in range(7):
+        f_rows.append(segment(0, g) * f_rows[-1] + segment(1, g))
+        b_rows.insert(0, segment(2, 7 - g) * b_rows[0] + segment(3, 7 - g))
+    f_in, b_in = jnp.concatenate(f_rows, axis=0), jnp.concatenate(b_rows, axis=0)
+
+    def states(s, held):
+        hf, hb = held
+        r = NS - 1 - s
+        hf = af[at(s), :] * hf + bf[at(s), :]
+        hb = ab[at(r), :] * hb + bb[at(r), :]
+        bf[at(s), :] = hf
+        bb[at(r), :] = hb
+        return hf, hb
+
+    lax.fori_loop(0, NS, states, (f_in, b_in), unroll=8)
+
+    def natural(s, _):
+        ynat[pl.ds(s, 8, stride=NS), :] = bf[at(s), :] + bb[at(s), :]
+        return 0
+
+    lax.fori_loop(0, NS, natural, 0, unroll=8)
+    loads[4].wait()
+
+    def finish(i, _):
+        rows = pl.ds(pl.multiple_of(i * CH, CH), CH)
+        rec_out[rows, :] = (ynat[rows, :] * jax.nn.gelu(gatev[rows, :].astype(F32))).astype(BF)
+        return 0
+
+    lax.fori_loop(0, S // CH, finish, 0)
 
     out = jnp.zeros((T * EXIT, LANES), F32)
     for w in range(2):
@@ -559,8 +557,8 @@
         rows,
         rows,
         pltpu.VMEM((4, 8, LANES), F32),
-        pltpu.VMEM((8, LANES), F32),
-        pltpu.VMEM((E, 8, LANES), F32),
+        pltpu.VMEM((2, 2, LANES), F32),
+        pltpu.VMEM((E, 2, LANES), F32),
         pltpu.VMEM((2, N, LANES), BF),
         pltpu.VMEM((2, NY, 2, N, LANES), BF),
         pltpu.VMEM((2, 2, N, F), F32),
@@ -599,7 +597,7 @@
             jax.ShapeDtypeStruct((S, LANES), BF),
             jax.ShapeDtypeStruct((EXIT, D), BF),
         ),
-        in_specs=[anywhere] * 6 + [vmem] * 9,
+        in_specs=[anywhere] * 6 + [vmem] * 8,
         out_specs=(vmem, vmem),
         scratch_shapes=scratch,
         compiler_params=pltpu.CompilerParams(
@@ -619,9 +617,8 @@
         decay_rate,
         decay_shift.reshape(8, S // 8),
         norm_gain.reshape(D // LANES, LANES),
-        routes,
         routes.T,
-        route_scores,
+        route_scores.T,
     )
 
 

time: 97.2 us -> 93.1 us (0.958)
  local copies, waits for them, and re-layouts: 4.61 us -> 2.33 us
  Pallas kernels: 91.8 us -> 89.9 us
    unnamed x10 -> x4, local copies, waits for them, and re-layouts: 4.61 us -> 2.33 us
    pallas_call x1, Pallas kernels: 91.8 us -> 89.9 us  [local(): pl.pallas_call(functools.partial(layer, E, T), out_shape=(jax.ShapeDtypeS...]
where the time goes in v2:
time: 93.1 us; the launch traced here: 92.9 us
  Pallas kernels  89.9 us (97%)
  local copies, waits for them, and re-layouts  2.33 us (3%)
    pallas_call x1, Pallas kernels, local(): pl.pallas_call(functools.partial(layer, E, T), out_shape=(jax.ShapeDtypeS...  89.9 us
    unnamed x4, local copies, waits for them, and re-layouts  2.33 us

profile of v2, /device:TPU:6, one launch (start us, length us, event | category | flops | bytes accessed | tf_op | source)
XLA Modules:
  0.0 92.9 jit_solution(18349380572995177396)
XLA Ops:
  0.6 89.9 %layer.1 = (bf16[1024,128]{1,0:T(8,128)(2,1)}, bf16[16,2048]{1,0:T(8,128)(2,1)}) custom-call(bf16[1024,128]{1,0:T(8,128)(2,1)} %x_hbm.1, bf16[1024,128]{1,0:T(8,128)(2,1)} %gate_hbm.1, bf16[256,2048]{1,0:T(8,128)(2,1)} %ein_hbm.1, bf16[2048,256]{1,0:T(8,128)(2,1)} %bitcast.7, bf16[2048,256]{1,0:T(8,128)(2,1)} %bitcast.8, bf16[256,2048]{1,0:T(8,128)(2,1)} %bitcast.9, ...), custom_call_target="tpu_custom_call" | custom-call | tf_op jit(solution)/shard_map/layer/pallas_call | solution.py:594
  90.5 0.0 copy-start
  90.5 1.7 %copy.18 = bf16[1024,128]{1,0:T(8,128)(2,1)} copy(bf16[1024,128]{1,0:T(8,128)(2,1)} %get-tuple-element.4) | data formatting | bytes 524288
  92.2 0.0 copy-done
  92.3 0.6 copy.19
Async XLA Ops:
  90.5 1.7 %copy-start = (bf16[16,2048]{1,0:T(8,128)(2,1)S(1)}, bf16[16,2048]{1,0:T(8,128)(2,1)}, u32[]{:S(2)}) copy-start(bf16[16,2048]{1,0:T(8,128)(2,1)} %get-tuple-element.5) | copy-start | bytes 196612

commit v3 on v2

v3 whole, which is shorter than its diff:
```python
import functools

import jax
import jax.numpy as jnp
from jax import lax
from jax.experimental import pallas as pl
from jax.experimental.pallas import tpu as pltpu
from jax.sharding import PartitionSpec as P

BF = jnp.bfloat16
F32 = jnp.float32
I32 = jnp.int32
MESH = pl.DeviceIdType.MESH
EPSILON = 1e-06
LANES = 128
EXIT = 16


def log2(n):
    return n.bit_length() - 1


def iota(shape, dim):
    return lax.broadcasted_iota(I32, shape, dim)


def shr(x, n):
    return lax.shift_right_logical(x, jnp.full(x.shape, n, I32))


def dot(a, b):
    return jnp.dot(a, b, preferred_element_type=F32)


def one_hot(mask):
    return jnp.where(mask, 1.0, 0.0).astype(BF)


def one_minus_square(log_a, a):
    z = 2.0 * log_a
    series = 1.0 + z * (1 / 2 + z * (1 / 6 + z * (1 / 24 + z * (1 / 120 + z * (1 / 720)))))
    return jnp.where(z > -0.25, -z * series, 1.0 - a * a)


def plane(E):
    X = 4 if E >= 32 else min(2, E)
    Z = E // X
    near = (
        [(0, 0), (0, 1), (0, 3), (1, 0), (7, 0), (1, 1), (7, 3), (0, 2)]
        + [(1, 3), (7, 1), (1, 2), (7, 2), (2, 0), (6, 0), (2, 1), (6, 3)]
        if E == 32
        else [(i // X, i % X) for i in range(E // 2)]
    )
    rest = [(z, x) for z in range(Z) for x in range(X) if (z, x) not in near]
    rest.sort(key=lambda p: -(min(p[0], Z - p[0]) + min(p[1], X - p[1])))
    return X, Z, near + rest


def layer(
    E,
    T,
    x_hbm,
    gate_hbm,
    ein_hbm,
    wg_hbm,
    wu_hbm,
    wd_hbm,
    taps,
    dgw,
    igw,
    rate,
    shift,
    gain,
    routes_t,
    scores_t,
    rec_out,
    exp_out,
    xraw,
    gatev,
    ein,
    wg,
    wu,
    wd,
    halo,
    xpad,
    sh,
    cperm,
    af,
    bf,
    ab,
    bb,
    ynat,
    seg,
    carry_send,
    carry_recv,
    named_as,
    far_select,
    near_select,
    normed,
    dsp,
    near_send,
    xb,
    xn,
    acc,
    perm,
    hp,
    part,
    pair,
    sums,
    came,
    stk,
    back,
    ret_recv,
    c_hi,
    c_lo,
    load_sem,
    halo_ss,
    halo_rs,
    carry_ss,
    carry_rs,
    dsp_ss,
    dsp_rs,
    near_ss,
    near_rs,
    mate_ss,
    mate_rs,
    ag_ss,
    ag_rs,
    sib_ss,
    sib_rs,
    sp_ss,
    sp_rs,
    rs_ss,
    rs_rs,
    ret_ss,
    ret_rs,
):
    NY, H, K, G = T // 2, T // 4, E // 2, E // 4
    S = xraw.shape[0]
    NS = S // 8
    R, D = ein.shape
    F = wg.shape[1]
    HALF = D // 2
    N, M, GT = E * T, K * T, G * T
    lT, lNY = log2(T), log2(NY)
    X, Z, slots = plane(E)

    e = lax.axis_index("ep")
    t = lax.axis_index("tp")
    y = t // 2
    c = t % 2
    sib_t = y * 2 + (1 - c)
    right_t = ((y + 1) % NY) * 2 + c
    left_t = ((y + NY - 1) % NY) * 2 + c
    ep_next = (e + 1) % E
    ep_prev = (e + E - 1) % E
    ez, ex = e // X, e % X

    def source_of(slot):
        dz, dx = slots[slot]
        return ((ez + dz) % Z) * X + (ex + dx) % X

    def target_of(slot):
        dz, dx = slots[slot]
        return ((ez + Z - dz) % Z) * X + (ex + X - dx) % X

    loads = [
        pltpu.make_async_copy(src, dst, load_sem.at[i])
        for i, (src, dst) in enumerate(
            ((ein_hbm, ein), (x_hbm, xraw), (wg_hbm, wg), (wu_hbm, wu), (gate_hbm, gatev), (wd_hbm, wd))
        )
    ]
    for load in loads:
        load.start()

    barrier = pltpu.get_barrier_semaphore()

    def greet(i, _):
        pl.semaphore_signal(barrier, inc=1, device_id=((e + i) % E, t), device_id_type=MESH)
        return 0

    lax.fori_loop(1, E, greet, 0)
    for peer in (sib_t, right_t, left_t):
        pl.semaphore_signal(barrier, inc=1, device_id=(e, peer), device_id_type=MESH)

    ids = iota((E, R), 0)
    first_t = routes_t[0:1, :] == ids
    second_t = routes_t[1:2, :] == ids
    named_t = one_hot(first_t | second_t)
    rr, rc = iota((R, R), 0), iota((R, R), 1)
    earlier_t = one_hot((shr(rr, 4) == shr(rc, 4)) & (rr < rc))
    rank_t = dot(named_t, earlier_t)
    for w in range(2):
        named_as[w] = jnp.where(rank_t == float(w), named_t.astype(F32), 0.0)
    in_block = iota((T, R), 0) == shr(iota((T, R), 1), 4)

    def selector(w, slot):
        named = named_as[w, pl.ds(target_of(slot), 1), :]
        return jnp.where(in_block, jnp.broadcast_to(named, (T, R)), 0.0).astype(BF)

    for w in range(2):
        for j in range(K):
            far_select[w, j * T : (j + 1) * T, :] = selector(w, K + j)
    loads[0].wait()
    total = jnp.zeros((R, LANES), F32)
    for j in range(D // LANES):
        tile = ein[:, j * LANES : (j + 1) * LANES].astype(F32)
        total = total + tile * tile
    scale = lax.rsqrt(jnp.sum(total, axis=1, keepdims=True) * (1.0 / D) + EPSILON)

    def normed_tile(j):
        columns = pl.ds(pl.multiple_of(j * LANES, LANES), LANES)
        return (ein[:, columns].astype(F32) * scale * gain[pl.ds(j, 1), :]).astype(BF)

    own_normed = normed_tile(t)
    for w in range(2):
        dsp[w] = dot(far_select[w], own_normed).astype(BF)

    loads[1].wait()
    pl.semaphore_wait(barrier, E + 2)

    tail = pltpu.make_async_remote_copy(
        xraw.at[pl.ds(S - EXIT, EXIT)], halo.at[0], halo_ss.at[0], halo_rs.at[0],
        device_id=(ep_next, t), device_id_type=MESH,
    )
    head = pltpu.make_async_remote_copy(
        xraw.at[pl.ds(0, EXIT)], halo.at[1], halo_ss.at[1], halo_rs.at[1],
        device_id=(ep_prev, t), device_id_type=MESH,
    )
    tail.start()
    head.start()

    own_rows = pl.ds(pl.multiple_of(e * T, T), T)
    for w in range(2):
        for j in range(K):
            rows = pl.ds(j * T, T)
            pltpu.make_async_remote_copy(
                dsp.at[w, rows], xb.at[w, y, c, rows], dsp_ss.at[w], dsp_rs.at[w],
                device_id=(target_of(K + j), t), device_id_type=MESH,
            ).start()

    for j in range(D // LANES):
        normed[:, j * LANES : (j + 1) * LANES] = normed_tile(j)
    for k in range(K):
        near_select[k * T : (k + 1) * T, :] = selector(c, k)
    near_send[...] = dot(near_select[...], normed[...]).astype(BF).reshape(2, GT, D)
    for k in range(K):
        g, rows = k // G, pl.ds(k % G * T, T)
        if k == 0:
            xn[g, c, rows, :] = near_send[g, rows, :]
            continue
        pltpu.make_async_remote_copy(
            near_send.at[g, rows], xn.at[g, c, rows], near_ss.at[g], near_rs.at[g],
            device_id=(target_of(k), t), device_id_type=MESH,
        ).start()

    n0, n1 = iota((M, M), 0), iota((M, M), 1)
    perm_block = (shr(n0, log2(K)) & (NY - 1)) * 2 + shr(n0, log2(K) + lNY)
    perm[...] = one_hot((shr(n1, lT) == (n0 & (K - 1))) & ((n1 & (T - 1)) == perm_block))

    xpad[pl.ds(EXIT, S), :] = xraw[...].astype(F32)
    for s in range(NS):
        sh[pl.ds(s * 8, 8), :] = jnp.broadcast_to(shift[:, s : s + 1], (8, LANES))
    tail.wait_recv()
    head.wait_recv()
    xpad[pl.ds(0, EXIT), :] = jnp.where(e > 0, halo[0].astype(F32), 0.0)
    xpad[pl.ds(EXIT + S, EXIT), :] = jnp.where(e < E - 1, halo[1].astype(F32), 0.0)

    def strided(s):
        return xpad[pl.ds(EXIT + s, 8, stride=NS), :]

    tap = [taps[k : k + 1, :] for k in range(4)]

    def conv(s, held):
        v0, v1, v2 = held
        v3 = strided(s + 1)
        value = v0 * tap[0] + v1 * tap[1] + v2 * tap[2] + v3 * tap[3]
        cperm[pl.ds(pl.multiple_of(s * 8, 8), 8), :] = value.astype(BF).astype(F32)
        return v1, v2, v3

    lax.fori_loop(0, NS, conv, (strided(-2), strided(-1), strided(0)), unroll=8)

    CH = min(128, S)

    def gates(i, _):
        rows = pl.ds(pl.multiple_of(i * CH, CH), CH)
        value = cperm[rows, :]
        value_b = value.astype(BF)
        shift_here = sh[rows, :]
        for d, (a_ref, b_ref) in enumerate(((af, bf), (ab, bb))):
            decay_gate = jax.nn.sigmoid(dot(value_b, dgw[d, 0]))
            input_gate = jax.nn.sigmoid(dot(value_b, igw[d, 0]))
            log_decay = -8.0 * decay_gate * rate[d : d + 1, :] + shift_here
            decay = jnp.exp(log_decay)
            rest = one_minus_square(log_decay, decay)
            root = rest * lax.rsqrt(jnp.maximum(rest, 1e-37))
            a_ref[rows, :] = decay
            b_ref[rows, :] = root * input_gate * value
        return 0

    lax.fori_loop(0, S // CH, gates, 0)

    def gather_copy(w, direction, hop):
        source = (y + NY - hop) % NY if direction == 0 else (y + hop) % NY
        block = xb.at[w, source, c, span(direction, hop)]
        return pltpu.make_async_remote_copy(
            block, block, ag_ss.at[w, direction, hop], ag_rs.at[w, direction, hop],
            device_id=(e, right_t if direction == 0 else left_t), device_id_type=MESH,
        )

    def span(direction, hop):
        return pl.ds(direction * (M // 2), M // 2) if hop == H - 1 else pl.ds(0, M)

    def arrived_gather(w, direction, hop):
        source = (y + 2 * NY - hop - 1) % NY if direction == 0 else (y + hop + 1) % NY
        block = xb.at[w, source, c, span(direction, hop)]
        pltpu.make_async_copy(block, block, ag_rs.at[w, direction, hop]).wait()

    def sibling_copy(w, source, index):
        block = xb.at[w, source, c]
        return pltpu.make_async_remote_copy(
            block, block, sib_ss.at[w, index], sib_rs.at[w, index],
            device_id=(e, sib_t), device_id_type=MESH,
        )

    def sibling_arrived(w, source, index):
        block = xb.at[w, source, 1 - c]
        pltpu.make_async_copy(block, block, sib_rs.at[w, index]).wait()

    def multiply(w, source, fresh):
        rows = jnp.concatenate([xb[w, source, 0], xb[w, source, 1]], axis=1)
        depth = pl.ds(pl.multiple_of(source * 2 * LANES, 2 * LANES), 2 * LANES)
        for k, weight in enumerate((wg, wu)):
            product = dot(rows, weight[depth, :])
            if fresh:
                acc[w, k] = product
            else:
                acc[w, k] += product

    for w in range(2):
        block = xb.at[w, y, c]
        pltpu.make_async_copy(block, block, dsp_rs.at[w]).wait()
        gather_copy(w, 0, 0).start()
        gather_copy(w, 1, 0).start()
        sibling_copy(w, y, 0).start()

    def turn(hop):
        return (y + NY - hop) % NY, (y + hop) % NY

    def multiply_hop(hop):
        for w in range(2):
            for k, source in enumerate(turn(hop) if hop else (y,)):
                index = 2 * hop - 1 + k if hop else 0
                sibling_arrived(w, source, index)
                multiply(w, source, hop == 0)

    far = (y + H) % NY

    def pair_copy(v, half):
        return pltpu.make_async_remote_copy(
            part.at[v, half, 1 - c], pair.at[v, half], sp_ss.at[v, half], sp_rs.at[v, half],
            device_id=(e, sib_t), device_id_type=MESH,
        )

    def down(v, hidden):
        hp[...] = dot(perm[...], hidden).astype(BF)
        for half in range(2):
            product = dot(hp[...], wd[:, half * HALF : (half + 1) * HALF]).astype(BF)
            part[v, half] = product.reshape(2, NY, K, HALF)
            pair_copy(v, half).start()

    def sum_copy(v, direction, step, half):
        return pltpu.make_async_remote_copy(
            sums.at[v, direction, step, half], came.at[v, direction, step, half],
            rs_ss.at[v, direction, step, half], rs_rs.at[v, direction, step, half],
            device_id=(e, right_t if direction == 0 else left_t), device_id_type=MESH,
        )

    def travels(direction, step, half):
        return step > 0 or half == direction

    def pair_sum(v, half, to):
        return part[v, half, c, to].astype(F32) + pair[v, half, to].astype(F32)

    def reduce_step(v, step):
        for half in range(2):
            if step == 0:
                pair_copy(v, half).wait_recv()
            for direction in range(2):
                if not travels(direction, step, half):
                    continue
                to = (y + H - step) % NY if direction == 0 else (y + NY - H + step) % NY
                value = pair_sum(v, half, to)
                if step > 0 and travels(direction, step - 1, half):
                    sum_copy(v, direction, step - 1, half).wait_recv()
                    value = value + came[v, direction, step - 1, half].astype(F32)
                sums[v, direction, step, half] = value.astype(BF)
                sum_copy(v, direction, step, half).start()

    def send_back(v):
        for half in range(2):
            value = pair_sum(v, half, y)
            for direction in range(2):
                if travels(direction, H - 1, half):
                    sum_copy(v, direction, H - 1, half).wait_recv()
                    value = value + came[v, direction, H - 1, half].astype(F32)
            for j in range(HALF // LANES):
                place = half * (HALF // LANES) + j
                stk[pl.ds(place, K, stride=T), :] = value[:, j * LANES : (j + 1) * LANES]
        back[v] = stk[...].astype(BF)
        for place in range(K):
            rows = pl.ds(place * T, T)
            w, slot = (v, K + place) if v < 2 else (place // G, (v - 2) * G + place % G)
            if slot == 0:
                ret_recv[w, own_rows] = back[v, rows, :]
            else:
                pltpu.make_async_remote_copy(
                    back.at[v, rows], ret_recv.at[w, own_rows], ret_ss.at[v], ret_rs.at[w],
                    device_id=(source_of(slot), t), device_id_type=MESH,
                ).start()

    def mate_copy(g):
        return pltpu.make_async_remote_copy(
            xn.at[g, c], xn.at[g, c], mate_ss.at[g], mate_rs.at[g],
            device_id=(e, sib_t), device_id_type=MESH,
        )

    def near_arrived(g):
        others = GT - T if g == 0 else GT
        if others:
            rows = xn.at[g, c, pl.ds(0, others)]
            pltpu.make_async_copy(rows, rows, near_rs.at[g]).wait()
        mate_copy(g).start()

    def near_wave(g):
        other = xn.at[g, 1 - c]
        pltpu.make_async_copy(other, other, mate_rs.at[g]).wait()
        rows = xn[g].reshape(M, D)
        hidden = jax.nn.silu(dot(rows, wg[...])) * dot(rows, wu[...])
        down(2 + g, hidden.astype(BF))

    def far_wave(w):
        sibling_arrived(w, far, NY - 1)
        multiply(w, far, False)
        down(w, (jax.nn.silu(acc[w, 0]) * acc[w, 1]).astype(BF))

    def gather_hop(hop):
        rights, lefts = turn(hop)
        for w in range(2):
            arrived_gather(w, 0, hop - 1)
            arrived_gather(w, 1, hop - 1)
            if hop == H:
                sibling_copy(w, far, NY - 1).start()
                continue
            gather_copy(w, 0, hop).start()
            gather_copy(w, 1, hop).start()
            sibling_copy(w, rights, 2 * hop - 1).start()
            sibling_copy(w, lefts, 2 * hop).start()

    def at(s):
        return pl.ds(pl.multiple_of(s * 8, 8), 8)

    def summing(s, held):
        hf, pf, hb, pb = held
        a, b = af[at(s), :], bf[at(s), :]
        a2, b2 = ab[at(NS - 1 - s), :], bb[at(NS - 1 - s), :]
        return a * hf + b, a * pf, a2 * hb + b2, a2 * pb

    zero, one = jnp.zeros((8, LANES), F32), jnp.ones((8, LANES), F32)
    hf, pf, hb, pb = lax.fori_loop(0, NS, summing, (zero, one, zero, one), unroll=8)
    for k, value in enumerate((pf, hf, pb, hb)):
        seg[k] = value

    def segment(k, g):
        return seg[k, g : g + 1, :]

    ones = jnp.ones((1, LANES), F32)
    fa, fb, ba, bb_ = ones, ones * 0.0, ones, ones * 0.0
    for g in range(8):
        fa, fb = segment(0, g) * fa, segment(0, g) * fb + segment(1, g)
        ba, bb_ = segment(2, 7 - g) * ba, segment(2, 7 - g) * bb_ + segment(3, 7 - g)
    ahead = jnp.concatenate([fa, fb], axis=0)
    behind = jnp.concatenate([ba, bb_], axis=0)
    carry_send[0] = ahead
    carry_send[1] = behind
    carry_recv[e] = ahead

    def send_carry(i, _):
        peer = (e + i) % E
        pltpu.make_async_remote_copy(
            carry_send.at[(peer < e).astype(I32)], carry_recv.at[e], carry_ss, carry_rs,
            device_id=(peer, t), device_id_type=MESH,
        ).start()
        return 0

    lax.fori_loop(1, E, send_carry, 0)

    near_arrived(0)
    loads[2].wait()
    loads[3].wait()
    loads[5].wait()
    for hop in range(1, H + 1):
        gather_hop(hop)
        if hop > 1 or H == 1:
            reduce_step(2, max(0, hop - 2))
        multiply_hop(hop - 1)
        if hop == 1:
            near_wave(0)
        if hop == max(1, H - 1):
            near_arrived(1)
    far_wave(0)
    far_wave(1)
    for step in range(max(1, H - 1), H):
        reduce_step(2, step)
    reduce_step(0, 0)
    reduce_step(1, 0)
    near_wave(1)
    for step in range(1, H):
        reduce_step(0, step)
        reduce_step(1, step)
        if step == 1:
            send_back(2)
        reduce_step(3, step - 1)
    send_back(0)
    send_back(1)
    reduce_step(3, H - 1)
    send_back(3)

    shares_t = scores_t[...] / (scores_t[0:1, :] + scores_t[1:2, :])
    share_of = jnp.where(first_t, shares_t[0:1, :], 0.0) + jnp.where(second_t, shares_t[1:2, :], 0.0)
    own_row = t * EXIT + (iota((T * EXIT, R), 0) & (EXIT - 1))
    rows_out = one_hot(own_row == iota((T * EXIT, R), 1))
    columns_out = one_hot(iota((E, N), 0) == shr(iota((E, N), 1), lT))
    same_tile = shr(iota((T * EXIT, N), 0), 4) == (iota((T * EXIT, N), 1) & (T - 1))
    for w in range(2):
        weight = jnp.where(rank_t == float(w), share_of, 0.0)
        high = weight.astype(BF)
        low = (weight - high.astype(F32)).astype(BF)
        for piece, table in ((high, c_hi), (low, c_lo)):
            picked = lax.dot_general(rows_out, piece, (((1,), (1,)), ((), ())), preferred_element_type=F32)
            wide = dot(picked.astype(BF), columns_out)
            table[w] = jnp.where(same_tile, wide, 0.0).astype(BF)

    pltpu.make_async_copy(
        carry_recv.at[pl.ds(0, E - 1)], carry_recv.at[pl.ds(0, E - 1)], carry_rs
    ).wait()

    def fold(i, held):
        f, b = held
        one_way = carry_recv[i]
        j = E - 1 - i
        other = carry_recv[j]
        f = jnp.where(i < e, one_way[0:1] * f + one_way[1:2], f)
        b = jnp.where(j > e, other[0:1] * b + other[1:2], b)
        return f, b

    f, b = lax.fori_loop(0, E, fold, (ones * 0.0, ones * 0.0))
    f_rows, b_rows = [f], [b]
    for g in range(7):
        f_rows.append(segment(0, g) * f_rows[-1] + segment(1, g))
        b_rows.insert(0, segment(2, 7 - g) * b_rows[0] + segment(3, 7 - g))
    f_in, b_in = jnp.concatenate(f_rows, axis=0), jnp.concatenate(b_rows, axis=0)

    def states(s, held):
        hf, hb = held
        r = NS - 1 - s
        hf = af[at(s), :] * hf + bf[at(s), :]
        hb = ab[at(r), :] * hb + bb[at(r), :]
        bf[at(s), :] = hf
        bb[at(r), :] = hb
        return hf, hb

    lax.fori_loop(0, NS, states, (f_in, b_in), unroll=8)

    def natural(s, _):
        ynat[pl.ds(s, 8, stride=NS), :] = bf[at(s), :] + bb[at(s), :]
        return 0

    lax.fori_loop(0, NS, natural, 0, unroll=8)
    loads[4].wait()

    def finish(i, _):
        rows = pl.ds(pl.multiple_of(i * CH, CH), CH)
        rec_out[rows, :] = (ynat[rows, :] * jax.nn.gelu(gatev[rows, :].astype(F32))).astype(BF)
        return 0

    lax.fori_loop(0, S // CH, finish, 0)

    arrivals = pl.ds(0, (E - 1) * T)
    out = jnp.zeros((T * EXIT, LANES), F32)
    for w in range(2):
        block = ret_recv.at[w, arrivals]
        pltpu.make_async_copy(block, block, ret_rs.at[w]).wait()
        out = out + dot(c_hi[w], ret_recv[w]) + dot(c_lo[w], ret_recv[w])
    for j in range(T):
        exp_out[:, j * LANES : (j + 1) * LANES] = out[j * EXIT : (j + 1) * EXIT, :].astype(BF)

    tail.wait_send()
    head.wait_send()
    sent = [(carry_recv.at[pl.ds(0, E - 1)], carry_ss), (near_send.at[1], near_ss.at[1])]
    sent += [(dsp.at[w], dsp_ss.at[w]) for w in range(2)]
    sent += [(back.at[v], ret_ss.at[v]) for v in (0, 1, 3)]
    if G > 1:
        sent += [(near_send.at[0, pl.ds(0, GT - T)], near_ss.at[0])]
        sent += [(back.at[2, pl.ds(0, M - 2 * T)], ret_ss.at[2])]
    for g in range(2):
        mate_copy(g).wait_send()
    for block, sem in sent:
        pltpu.make_async_copy(block, block, sem).wait()
    for w in range(2):
        for hop in range(H):
            for direction in range(2):
                gather_copy(w, direction, hop).wait_send()
        for index in range(NY):
            sibling_copy(w, y, index).wait_send()
    for v in range(4):
        for half in range(2):
            pair_copy(v, half).wait_send()
            for direction in range(2):
                for step in range(H):
                    if travels(direction, step, half):
                        sum_copy(v, direction, step, half).wait_send()


def local(
    E, T, x_path, gate_path, conv_taps, decay_gate_w, input_gate_w, decay_rate, decay_shift,
    expert_in, norm_gain, routes, route_scores, gate_weight, up_weight, down_weight,
):
    S = x_path.shape[0]
    R, D = expert_in.shape
    F = gate_weight.shape[2]
    NY, H, K, HALF = T // 2, T // 4, E // 2, D // 2
    N, M = E * T, K * T
    anywhere = pl.BlockSpec(memory_space=pl.ANY)
    vmem = pl.BlockSpec(memory_space=pltpu.VMEM)
    dma = pltpu.SemaphoreType.DMA
    rows = pltpu.VMEM((S, LANES), F32)
    scratch = [
        pltpu.VMEM((S, LANES), BF),
        pltpu.VMEM((S, LANES), BF),
        pltpu.VMEM((R, D), BF),
        pltpu.VMEM((D, F), BF),
        pltpu.VMEM((D, F), BF),
        pltpu.VMEM((F, D), BF),
        pltpu.VMEM((2, EXIT, LANES), BF),
        pltpu.VMEM((S + 2 * EXIT, LANES), F32),
        rows,
        rows,
        rows,
        rows,
        rows,
        rows,
        rows,
        pltpu.VMEM((4, 8, LANES), F32),
        pltpu.VMEM((2, 2, LANES), F32),
        pltpu.VMEM((E, 2, LANES), F32),
        pltpu.VMEM((2, E, R), F32),
        pltpu.VMEM((2, M, R), BF),
        pltpu.VMEM((M, R), BF),
        pltpu.VMEM((R, D), BF),
        pltpu.VMEM((2, M, LANES), BF),
        pltpu.VMEM((2, M // 2, D), BF),
        pltpu.VMEM((2, NY, 2, M, LANES), BF),
        pltpu.VMEM((2, 2, M // 2, D), BF),
        pltpu.VMEM((2, 2, M, F), F32),
        pltpu.VMEM((M, M), BF),
        pltpu.VMEM((M, F), BF),
        pltpu.VMEM((4, 2, 2, NY, K, HALF), BF),
        pltpu.VMEM((4, 2, NY, K, HALF), BF),
        pltpu.VMEM((4, 2, H, 2, K, HALF), BF),
        pltpu.VMEM((4, 2, H, 2, K, HALF), BF),
        pltpu.VMEM((M, LANES), F32),
        pltpu.VMEM((4, M, LANES), BF),
        pltpu.VMEM((2, N, LANES), BF),
        pltpu.VMEM((2, T * EXIT, N), BF),
        pltpu.VMEM((2, T * EXIT, N), BF),
        dma((6,)),
        dma((2,)),
        dma((2,)),
        dma,
        dma,
        dma((2,)),
        dma((2,)),
        dma((2,)),
        dma((2,)),
        dma((2,)),
        dma((2,)),
        dma((2, 2, H)),
        dma((2, 2, H)),
        dma((2, NY)),
        dma((2, NY)),
        dma((4, 2)),
        dma((4, 2)),
        dma((4, 2, H, 2)),
        dma((4, 2, H, 2)),
        dma((4,)),
        dma((2,)),
    ]
    return pl.pallas_call(
        functools.partial(layer, E, T),
        out_shape=(
            jax.ShapeDtypeStruct((S, LANES), BF),
            jax.ShapeDtypeStruct((EXIT, D), BF),
        ),
        in_specs=[anywhere] * 6 + [vmem] * 8,
        out_specs=(vmem, vmem),
        scratch_shapes=scratch,
        compiler_params=pltpu.CompilerParams(
            collective_id=0, has_side_effects=True, vmem_limit_bytes=60 * 1024 * 1024
        ),
        name="layer",
    )(
        x_path,
        gate_path,
        expert_in,
        gate_weight.reshape(D, F),
        up_weight.reshape(D, F),
        down_weight.reshape(F, D),
        conv_taps,
        decay_gate_w,
        input_gate_w,
        decay_rate,
        decay_shift.reshape(8, S // 8),
        norm_gain.reshape(D // LANES, LANES),
        routes.T,
        route_scores.T,
    )


def solution(mesh):
    in_specs = (
        P("ep", "tp"),
        P("ep", "tp"),
        P(None, "tp"),
        P(None, "tp", None, None),
        P(None, "tp", None, None),
        P(None, "tp"),
        P("ep", "tp"),
        P("ep", None),
        P(),
        P("ep", None),
        P("ep", None),
        P("ep", None, "tp"),
        P("ep", None, "tp"),
        P("ep", "tp", None),
    )
    out_specs = (P("ep", "tp"), P(("ep", "tp"), None))
    step = functools.partial(local, mesh.shape["ep"], mesh.shape["tp"])
    return jax.shard_map(step, mesh=mesh, in_specs=in_specs, out_specs=out_specs, check_vma=False)
```

time: 93.1 us -> 77.4 us (0.83); the launches traced: 92.9 us -> 76.1 us
  Pallas kernels: 89.9 us -> 73.1 us
    pallas_call x1, Pallas kernels: 89.9 us -> 73.1 us  [local(): pl.pallas_call(functools.partial(layer, E, T), out_shape=(jax.ShapeDtypeS...]
where the time goes in v3:
time: 77.4 us; the launch traced here: 76.1 us
  Pallas kernels  73.1 us (94%)
  local copies, waits for them, and re-layouts  2.33 us (3%)
    pallas_call x1, Pallas kernels, local(): pl.pallas_call(functools.partial(layer, E, T), out_shape=(jax.ShapeDtypeS...  73.1 us
    unnamed x4, local copies, waits for them, and re-layouts  2.33 us

profile of v3, /device:TPU:6, one launch (start us, length us, event | category | flops | bytes accessed | tf_op | source)
XLA Modules:
  0.0 76.1 jit_solution(1085581083324725641)
XLA Ops:
  0.6 73.1 %layer.1 = (bf16[1024,128]{1,0:T(8,128)(2,1)}, bf16[16,2048]{1,0:T(8,128)(2,1)}) custom-call(bf16[1024,128]{1,0:T(8,128)(2,1)} %x_hbm.1, bf16[1024,128]{1,0:T(8,128)(2,1)} %gate_hbm.1, bf16[256,2048]{1,0:T(8,128)(2,1)} %ein_hbm.1, bf16[2048,256]{1,0:T(8,128)(2,1)} %bitcast.7, bf16[2048,256]{1,0:T(8,128)(2,1)} %bitcast.8, bf16[256,2048]{1,0:T(8,128)(2,1)} %bitcast.9, ...), custom_call_target="tpu_custom_call" | custom-call | tf_op jit(solution)/shard_map/layer/pallas_call | solution.py:699
  73.8 0.0 copy-start
  73.8 1.7 %copy.18 = bf16[1024,128]{1,0:T(8,128)(2,1)} copy(bf16[1024,128]{1,0:T(8,128)(2,1)} %get-tuple-element.4) | data formatting | bytes 524288
  75.5 0.0 copy-done
  75.5 0.6 copy.19
Async XLA Ops:
  73.8 1.7 %copy-start = (bf16[16,2048]{1,0:T(8,128)(2,1)S(1)}, bf16[16,2048]{1,0:T(8,128)(2,1)}, u32[]{:S(2)}) copy-start(bf16[16,2048]{1,0:T(8,128)(2,1)} %get-tuple-element.5) | copy-start | bytes 196612

commit v4 on v3

--- a/solution.py
+++ b/solution.py
@@ -65,6 +65,22 @@
     wg_hbm,
     wu_hbm,
     wd_hbm,
+    taps_hbm,
+    dgw_hbm,
+    igw_hbm,
+    rate_hbm,
+    shift_hbm,
+    gain_hbm,
+    routes_hbm,
+    scores_hbm,
+    rec_hbm,
+    exp_hbm,
+    xraw,
+    gatev,
+    ein,
+    wg,
+    wu,
+    wd,
     taps,
     dgw,
     igw,
@@ -75,12 +91,6 @@
     scores_t,
     rec_out,
     exp_out,
-    xraw,
-    gatev,
-    ein,
-    wg,
-    wu,
-    wd,
     halo,
     xpad,
     sh,
@@ -114,6 +124,7 @@
     c_hi,
     c_lo,
     load_sem,
+    store_sem,
     halo_ss,
     halo_rs,
     carry_ss,
@@ -164,25 +175,41 @@
         dz, dx = slots[slot]
         return ((ez + Z - dz) % Z) * X + (ex + X - dx) % X
 
-    loads = [
-        pltpu.make_async_copy(src, dst, load_sem.at[i])
-        for i, (src, dst) in enumerate(
-            ((ein_hbm, ein), (x_hbm, xraw), (wg_hbm, wg), (wu_hbm, wu), (gate_hbm, gatev), (wd_hbm, wd))
-        )
+    barrier = pltpu.get_barrier_semaphore()
+
+    greeted = list(range(K)) + list(range(E - 1, K - 1, -1))
+
+    pairs = (
+        (routes_hbm, routes_t),
+        (ein_hbm, ein),
+        (gain_hbm, gain),
+        (x_hbm, xraw),
+        (taps_hbm, taps),
+        (shift_hbm, shift),
+        (rate_hbm, rate),
+        (dgw_hbm, dgw),
+        (igw_hbm, igw),
+        (scores_hbm, scores_t),
+        (wg_hbm, wg),
+        (wu_hbm, wu),
+        (wd_hbm, wd),
+        (gate_hbm, gatev),
+    )
+    loads = [pltpu.make_async_copy(src, dst, load_sem.at[i]) for i, (src, dst) in enumerate(pairs)]
+    stores = [
+        pltpu.make_async_copy(rec_out, rec_hbm, store_sem.at[0]),
+        pltpu.make_async_copy(exp_out, exp_hbm, store_sem.at[1]),
     ]
-    for load in loads:
+    for load in loads[:4]:
         load.start()
-
-    barrier = pltpu.get_barrier_semaphore()
-
-    def greet(i, _):
-        pl.semaphore_signal(barrier, inc=1, device_id=((e + i) % E, t), device_id_type=MESH)
-        return 0
-
-    lax.fori_loop(1, E, greet, 0)
+    for slot in range(E - 1, 0, -1):
+        pl.semaphore_signal(barrier, inc=1, device_id=(target_of(greeted[slot]), t), device_id_type=MESH)
     for peer in (sib_t, right_t, left_t):
         pl.semaphore_signal(barrier, inc=1, device_id=(e, peer), device_id_type=MESH)
-
+    for load in loads[4:]:
+        load.start()
+
+    loads[0].wait()
     ids = iota((E, R), 0)
     first_t = routes_t[0:1, :] == ids
     second_t = routes_t[1:2, :] == ids
@@ -201,7 +228,8 @@
     for w in range(2):
         for j in range(K):
             far_select[w, j * T : (j + 1) * T, :] = selector(w, K + j)
-    loads[0].wait()
+    loads[1].wait()
+    loads[2].wait()
     total = jnp.zeros((R, LANES), F32)
     for j in range(D // LANES):
         tile = ein[:, j * LANES : (j + 1) * LANES].astype(F32)
@@ -216,7 +244,7 @@
     for w in range(2):
         dsp[w] = dot(far_select[w], own_normed).astype(BF)
 
-    loads[1].wait()
+    loads[3].wait()
     pl.semaphore_wait(barrier, E + 2)
 
     tail = pltpu.make_async_remote_copy(
@@ -244,20 +272,26 @@
     for k in range(K):
         near_select[k * T : (k + 1) * T, :] = selector(c, k)
     near_send[...] = dot(near_select[...], normed[...]).astype(BF).reshape(2, GT, D)
-    for k in range(K):
-        g, rows = k // G, pl.ds(k % G * T, T)
-        if k == 0:
-            xn[g, c, rows, :] = near_send[g, rows, :]
-            continue
-        pltpu.make_async_remote_copy(
-            near_send.at[g, rows], xn.at[g, c, rows], near_ss.at[g], near_rs.at[g],
-            device_id=(target_of(k), t), device_id_type=MESH,
-        ).start()
+
+    def send_near(g):
+        for k in range(G):
+            rows = pl.ds(k * T, T)
+            if g + k == 0:
+                xn[g, c, rows, :] = near_send[g, rows, :]
+                continue
+            pltpu.make_async_remote_copy(
+                near_send.at[g, rows], xn.at[g, c, rows], near_ss.at[g], near_rs.at[g],
+                device_id=(target_of(g * G + k), t), device_id_type=MESH,
+            ).start()
+
+    send_near(0)
 
     n0, n1 = iota((M, M), 0), iota((M, M), 1)
     perm_block = (shr(n0, log2(K)) & (NY - 1)) * 2 + shr(n0, log2(K) + lNY)
     perm[...] = one_hot((shr(n1, lT) == (n0 & (K - 1))) & ((n1 & (T - 1)) == perm_block))
 
+    for load in loads[4:9]:
+        load.wait()
     xpad[pl.ds(EXIT, S), :] = xraw[...].astype(F32)
     for s in range(NS):
         sh[pl.ds(s * 8, 8), :] = jnp.broadcast_to(shift[:, s : s + 1], (8, LANES))
@@ -279,26 +313,6 @@
         return v1, v2, v3
 
     lax.fori_loop(0, NS, conv, (strided(-2), strided(-1), strided(0)), unroll=8)
-
-    CH = min(128, S)
-
-    def gates(i, _):
-        rows = pl.ds(pl.multiple_of(i * CH, CH), CH)
-        value = cperm[rows, :]
-        value_b = value.astype(BF)
-        shift_here = sh[rows, :]
-        for d, (a_ref, b_ref) in enumerate(((af, bf), (ab, bb))):
-            decay_gate = jax.nn.sigmoid(dot(value_b, dgw[d, 0]))
-            input_gate = jax.nn.sigmoid(dot(value_b, igw[d, 0]))
-            log_decay = -8.0 * decay_gate * rate[d : d + 1, :] + shift_here
-            decay = jnp.exp(log_decay)
-            rest = one_minus_square(log_decay, decay)
-            root = rest * lax.rsqrt(jnp.maximum(rest, 1e-37))
-            a_ref[rows, :] = decay
-            b_ref[rows, :] = root * input_gate * value
-        return 0
-
-    lax.fori_loop(0, S // CH, gates, 0)
 
     def gather_copy(w, direction, hop):
         source = (y + NY - hop) % NY if direction == 0 else (y + hop) % NY
@@ -337,6 +351,7 @@
             else:
                 acc[w, k] += product
 
+    send_near(1)
     for w in range(2):
         block = xb.at[w, y, c]
         pltpu.make_async_copy(block, block, dsp_rs.at[w]).wait()
@@ -347,12 +362,11 @@
     def turn(hop):
         return (y + NY - hop) % NY, (y + hop) % NY
 
-    def multiply_hop(hop):
-        for w in range(2):
-            for k, source in enumerate(turn(hop) if hop else (y,)):
-                index = 2 * hop - 1 + k if hop else 0
-                sibling_arrived(w, source, index)
-                multiply(w, source, hop == 0)
+    def multiply_hop(hop, w):
+        for k, source in enumerate(turn(hop) if hop else (y,)):
+            index = 2 * hop - 1 + k if hop else 0
+            sibling_arrived(w, source, index)
+            multiply(w, source, hop == 0)
 
     far = (y + H) % NY
 
@@ -444,18 +458,38 @@
         multiply(w, far, False)
         down(w, (jax.nn.silu(acc[w, 0]) * acc[w, 1]).astype(BF))
 
-    def gather_hop(hop):
+    def gather_hop(hop, w):
         rights, lefts = turn(hop)
-        for w in range(2):
-            arrived_gather(w, 0, hop - 1)
-            arrived_gather(w, 1, hop - 1)
-            if hop == H:
-                sibling_copy(w, far, NY - 1).start()
-                continue
+        arrived_gather(w, 0, hop - 1)
+        if hop < H:
             gather_copy(w, 0, hop).start()
+        arrived_gather(w, 1, hop - 1)
+        if hop < H:
             gather_copy(w, 1, hop).start()
             sibling_copy(w, rights, 2 * hop - 1).start()
             sibling_copy(w, lefts, 2 * hop).start()
+        else:
+            sibling_copy(w, far, NY - 1).start()
+
+    CH = min(128, S)
+
+    def gates(i, _):
+        rows = pl.ds(pl.multiple_of(i * CH, CH), CH)
+        value = cperm[rows, :]
+        value_b = value.astype(BF)
+        shift_here = sh[rows, :]
+        for d, (a_ref, b_ref) in enumerate(((af, bf), (ab, bb))):
+            decay_gate = jax.nn.sigmoid(dot(value_b, dgw[d, 0]))
+            input_gate = jax.nn.sigmoid(dot(value_b, igw[d, 0]))
+            log_decay = -8.0 * decay_gate * rate[d : d + 1, :] + shift_here
+            decay = jnp.exp(log_decay)
+            rest = one_minus_square(log_decay, decay)
+            root = rest * lax.rsqrt(jnp.maximum(rest, 1e-37))
+            a_ref[rows, :] = decay
+            b_ref[rows, :] = root * input_gate * value
+        return 0
+
+    lax.fori_loop(0, S // CH, gates, 0)
 
     def at(s):
         return pl.ds(pl.multiple_of(s * 8, 8), 8)
@@ -495,37 +529,90 @@
 
     lax.fori_loop(1, E, send_carry, 0)
 
+    def second_pass():
+        pltpu.make_async_copy(
+            carry_recv.at[pl.ds(0, E - 1)], carry_recv.at[pl.ds(0, E - 1)], carry_rs
+        ).wait()
+
+        def fold(i, held):
+            f, b = held
+            one_way = carry_recv[i]
+            j = E - 1 - i
+            other = carry_recv[j]
+            f = jnp.where(i < e, one_way[0:1] * f + one_way[1:2], f)
+            b = jnp.where(j > e, other[0:1] * b + other[1:2], b)
+            return f, b
+
+        f, b = lax.fori_loop(0, E, fold, (ones * 0.0, ones * 0.0))
+        f_rows, b_rows = [f], [b]
+        for g in range(7):
+            f_rows.append(segment(0, g) * f_rows[-1] + segment(1, g))
+            b_rows.insert(0, segment(2, 7 - g) * b_rows[0] + segment(3, 7 - g))
+        f_in, b_in = jnp.concatenate(f_rows, axis=0), jnp.concatenate(b_rows, axis=0)
+
+        def states(s, held):
+            hf, hb = held
+            r = NS - 1 - s
+            hf = af[at(s), :] * hf + bf[at(s), :]
+            hb = ab[at(r), :] * hb + bb[at(r), :]
+            bf[at(s), :] = hf
+            bb[at(r), :] = hb
+            return hf, hb
+
+        lax.fori_loop(0, NS, states, (f_in, b_in), unroll=8)
+
+        def natural(s, _):
+            ynat[pl.ds(s, 8, stride=NS), :] = bf[at(s), :] + bb[at(s), :]
+            return 0
+
+        lax.fori_loop(0, NS, natural, 0, unroll=8)
+        loads[13].wait()
+
+        def finish(i, _):
+            rows = pl.ds(pl.multiple_of(i * CH, CH), CH)
+            rec_out[rows, :] = (ynat[rows, :] * jax.nn.gelu(gatev[rows, :].astype(F32))).astype(BF)
+            return 0
+
+        lax.fori_loop(0, S // CH, finish, 0)
+        stores[0].start()
+
     near_arrived(0)
-    loads[2].wait()
-    loads[3].wait()
-    loads[5].wait()
-    for hop in range(1, H + 1):
-        gather_hop(hop)
-        if hop > 1 or H == 1:
-            reduce_step(2, max(0, hop - 2))
-        multiply_hop(hop - 1)
+    for load in loads[10:13]:
+        load.wait()
+    for hop in range(1, H):
+        for w in range(2):
+            gather_hop(hop, w)
+        if hop == H - 1:
+            near_arrived(1)
+        if hop > 1:
+            reduce_step(2, hop - 2)
+        for w in range(2):
+            multiply_hop(hop - 1, w)
         if hop == 1:
             near_wave(0)
-        if hop == max(1, H - 1):
-            near_arrived(1)
+    near_wave(1)
+    for w in range(2):
+        gather_hop(H, w)
+        multiply_hop(H - 1, w)
+    reduce_step(2, H - 2)
+    reduce_step(3, 0)
     far_wave(0)
     far_wave(1)
-    for step in range(max(1, H - 1), H):
-        reduce_step(2, step)
     reduce_step(0, 0)
+    reduce_step(2, H - 1)
     reduce_step(1, 0)
-    near_wave(1)
+    reduce_step(3, 1)
     for step in range(1, H):
         reduce_step(0, step)
         reduce_step(1, step)
         if step == 1:
             send_back(2)
-        reduce_step(3, step - 1)
+        if step + 1 < H:
+            reduce_step(3, step + 1)
+    send_back(3)
     send_back(0)
     send_back(1)
-    reduce_step(3, H - 1)
-    send_back(3)
-
+    loads[9].wait()
     shares_t = scores_t[...] / (scores_t[0:1, :] + scores_t[1:2, :])
     share_of = jnp.where(first_t, shares_t[0:1, :], 0.0) + jnp.where(second_t, shares_t[1:2, :], 0.0)
     own_row = t * EXIT + (iota((T * EXIT, R), 0) & (EXIT - 1))
@@ -541,51 +628,7 @@
             wide = dot(picked.astype(BF), columns_out)
             table[w] = jnp.where(same_tile, wide, 0.0).astype(BF)
 
-    pltpu.make_async_copy(
-        carry_recv.at[pl.ds(0, E - 1)], carry_recv.at[pl.ds(0, E - 1)], carry_rs
-    ).wait()
-
-    def fold(i, held):
-        f, b = held
-        one_way = carry_recv[i]
-        j = E - 1 - i
-        other = carry_recv[j]
-        f = jnp.where(i < e, one_way[0:1] * f + one_way[1:2], f)
-        b = jnp.where(j > e, other[0:1] * b + other[1:2], b)
-        return f, b
-
-    f, b = lax.fori_loop(0, E, fold, (ones * 0.0, ones * 0.0))
-    f_rows, b_rows = [f], [b]
-    for g in range(7):
-        f_rows.append(segment(0, g) * f_rows[-1] + segment(1, g))
-        b_rows.insert(0, segment(2, 7 - g) * b_rows[0] + segment(3, 7 - g))
-    f_in, b_in = jnp.concatenate(f_rows, axis=0), jnp.concatenate(b_rows, axis=0)
-
-    def states(s, held):
-        hf, hb = held
-        r = NS - 1 - s
-        hf = af[at(s), :] * hf + bf[at(s), :]
-        hb = ab[at(r), :] * hb + bb[at(r), :]
-        bf[at(s), :] = hf
-        bb[at(r), :] = hb
-        return hf, hb
-
-    lax.fori_loop(0, NS, states, (f_in, b_in), unroll=8)
-
-    def natural(s, _):
-        ynat[pl.ds(s, 8, stride=NS), :] = bf[at(s), :] + bb[at(s), :]
-        return 0
-
-    lax.fori_loop(0, NS, natural, 0, unroll=8)
-    loads[4].wait()
-
-    def finish(i, _):
-        rows = pl.ds(pl.multiple_of(i * CH, CH), CH)
-        rec_out[rows, :] = (ynat[rows, :] * jax.nn.gelu(gatev[rows, :].astype(F32))).astype(BF)
-        return 0
-
-    lax.fori_loop(0, S // CH, finish, 0)
-
+    second_pass()
     arrivals = pl.ds(0, (E - 1) * T)
     out = jnp.zeros((T * EXIT, LANES), F32)
     for w in range(2):
@@ -594,6 +637,7 @@
         out = out + dot(c_hi[w], ret_recv[w]) + dot(c_lo[w], ret_recv[w])
     for j in range(T):
         exp_out[:, j * LANES : (j + 1) * LANES] = out[j * EXIT : (j + 1) * EXIT, :].astype(BF)
+    stores[1].start()
 
     tail.wait_send()
     head.wait_send()
@@ -620,6 +664,8 @@
                 for step in range(H):
                     if travels(direction, step, half):
                         sum_copy(v, direction, step, half).wait_send()
+    for store in stores:
+        store.wait()
 
 
 def local(
@@ -631,8 +677,7 @@
     F = gate_weight.shape[2]
     NY, H, K, HALF = T // 2, T // 4, E // 2, D // 2
     N, M = E * T, K * T
-    anywhere = pl.BlockSpec(memory_space=pl.ANY)
-    vmem = pl.BlockSpec(memory_space=pltpu.VMEM)
+    hbm = pl.BlockSpec(memory_space=pltpu.HBM)
     dma = pltpu.SemaphoreType.DMA
     rows = pltpu.VMEM((S, LANES), F32)
     scratch = [
@@ -642,6 +687,16 @@
         pltpu.VMEM((D, F), BF),
         pltpu.VMEM((D, F), BF),
         pltpu.VMEM((F, D), BF),
+        pltpu.VMEM((4, LANES), F32),
+        pltpu.VMEM((2, 1, LANES, LANES), BF),
+        pltpu.VMEM((2, 1, LANES, LANES), BF),
+        pltpu.VMEM((2, LANES), F32),
+        pltpu.VMEM((8, S // 8), F32),
+        pltpu.VMEM((D // LANES, LANES), F32),
+        pltpu.VMEM((2, R), I32),
+        pltpu.VMEM((2, R), F32),
+        pltpu.VMEM((S, LANES), BF),
+        pltpu.VMEM((EXIT, D), BF),
         pltpu.VMEM((2, EXIT, LANES), BF),
         pltpu.VMEM((S + 2 * EXIT, LANES), F32),
         rows,
@@ -674,7 +729,8 @@
         pltpu.VMEM((2, N, LANES), BF),
         pltpu.VMEM((2, T * EXIT, N), BF),
         pltpu.VMEM((2, T * EXIT, N), BF),
-        dma((6,)),
+        dma((14,)),
+        dma((2,)),
         dma((2,)),
         dma((2,)),
         dma,
@@ -702,8 +758,8 @@
             jax.ShapeDtypeStruct((S, LANES), BF),
             jax.ShapeDtypeStruct((EXIT, D), BF),
         ),
-        in_specs=[anywhere] * 6 + [vmem] * 8,
-        out_specs=(vmem, vmem),
+        in_specs=[hbm] * 14,
+        out_specs=(hbm, hbm),
         scratch_shapes=scratch,
         compiler_params=pltpu.CompilerParams(
             collective_id=0, has_side_effects=True, vmem_limit_bytes=60 * 1024 * 1024

time: 77.4 us -> 73.5 us (0.950)
  Pallas kernels: 73.1 us -> 69.4 us
    pallas_call x1, Pallas kernels: 73.1 us -> 69.4 us  [local(): pl.pallas_call(functools.partial(layer, E, T), out_shape=(jax.ShapeDtypeS...]
where the time goes in v4:
time: 73.5 us; the launch traced here: 72.4 us
  Pallas kernels  69.4 us (94%)
  local copies, waits for them, and re-layouts  2.33 us (3%)
    pallas_call x1, Pallas kernels, local(): pl.pallas_call(functools.partial(layer, E, T), out_shape=(jax.ShapeDtypeS...  69.4 us
    unnamed x4, local copies, waits for them, and re-layouts  2.33 us

profile of v4, /device:TPU:6, one launch (start us, length us, event | category | flops | bytes accessed | tf_op | source)
XLA Modules:
  0.0 72.4 jit_solution(10758992374752903903)
XLA Ops:
  0.6 69.4 %layer.1 = (bf16[1024,128]{1,0:T(8,128)(2,1)}, bf16[16,2048]{1,0:T(8,128)(2,1)}) custom-call(bf16[1024,128]{1,0:T(8,128)(2,1)} %x_hbm.1, bf16[1024,128]{1,0:T(8,128)(2,1)} %gate_hbm.1, bf16[256,2048]{1,0:T(8,128)(2,1)} %ein_hbm.1, bf16[2048,256]{1,0:T(8,128)(2,1)} %bitcast.7, bf16[2048,256]{1,0:T(8,128)(2,1)} %bitcast.8, bf16[256,2048]{1,0:T(8,128)(2,1)} %bitcast.9, ...), custom_call_target="tpu_custom_call" | custom-call | tf_op jit(solution)/shard_map/layer/pallas_call | solution.py:755
  70.1 0.0 copy-start
  70.1 1.7 %copy.18 = bf16[1024,128]{1,0:T(8,128)(2,1)} copy(bf16[1024,128]{1,0:T(8,128)(2,1)} %get-tuple-element.4) | data formatting | bytes 524288
  71.8 0.0 copy-done
  71.8 0.6 copy.19
Async XLA Ops:
  70.1 1.7 %copy-start = (bf16[16,2048]{1,0:T(8,128)(2,1)S(1)}, bf16[16,2048]{1,0:T(8,128)(2,1)}, u32[]{:S(2)}) copy-start(bf16[16,2048]{1,0:T(8,128)(2,1)} %get-tuple-element.5) | copy-start | bytes 196612

commit v5 on v4

--- a/solution.py
+++ b/solution.py
@@ -280,7 +280,7 @@
                 xn[g, c, rows, :] = near_send[g, rows, :]
                 continue
             pltpu.make_async_remote_copy(
-                near_send.at[g, rows], xn.at[g, c, rows], near_ss.at[g], near_rs.at[g],
+                near_send.at[g, rows], xn.at[g, c, rows], near_ss.at[g], near_rs.at[g, k],
                 device_id=(target_of(g * G + k), t), device_id_type=MESH,
             ).start()
 
@@ -313,6 +313,26 @@
         return v1, v2, v3
 
     lax.fori_loop(0, NS, conv, (strided(-2), strided(-1), strided(0)), unroll=8)
+
+    CH = min(128, S)
+
+    def gates(i, _):
+        rows = pl.ds(pl.multiple_of(i * CH, CH), CH)
+        value = cperm[rows, :]
+        value_b = value.astype(BF)
+        shift_here = sh[rows, :]
+        for d, (a_ref, b_ref) in enumerate(((af, bf), (ab, bb))):
+            decay_gate = jax.nn.sigmoid(dot(value_b, dgw[d, 0]))
+            input_gate = jax.nn.sigmoid(dot(value_b, igw[d, 0]))
+            log_decay = -8.0 * decay_gate * rate[d : d + 1, :] + shift_here
+            decay = jnp.exp(log_decay)
+            rest = one_minus_square(log_decay, decay)
+            root = rest * lax.rsqrt(jnp.maximum(rest, 1e-37))
+            a_ref[rows, :] = decay
+            b_ref[rows, :] = root * input_gate * value
+        return 0
+
+    lax.fori_loop(0, S // CH, gates, 0)
 
     def gather_copy(w, direction, hop):
         source = (y + NY - hop) % NY if direction == 0 else (y + hop) % NY
@@ -433,18 +453,14 @@
                     device_id=(source_of(slot), t), device_id_type=MESH,
                 ).start()
 
-    def mate_copy(g):
-        return pltpu.make_async_remote_copy(
-            xn.at[g, c], xn.at[g, c], mate_ss.at[g], mate_rs.at[g],
-            device_id=(e, sib_t), device_id_type=MESH,
-        )
-
-    def near_arrived(g):
-        others = GT - T if g == 0 else GT
-        if others:
-            rows = xn.at[g, c, pl.ds(0, others)]
-            pltpu.make_async_copy(rows, rows, near_rs.at[g]).wait()
-        mate_copy(g).start()
+    def near_arrived(g, first, last):
+        for k in range(first, last):
+            rows = xn.at[g, c, pl.ds(k * T, T)]
+            if g + k:
+                pltpu.make_async_copy(rows, rows, near_rs.at[g, k]).wait()
+            pltpu.make_async_remote_copy(
+                rows, rows, mate_ss.at[g], mate_rs.at[g], device_id=(e, sib_t), device_id_type=MESH
+            ).start()
 
     def near_wave(g):
         other = xn.at[g, 1 - c]
@@ -471,26 +487,6 @@
         else:
             sibling_copy(w, far, NY - 1).start()
 
-    CH = min(128, S)
-
-    def gates(i, _):
-        rows = pl.ds(pl.multiple_of(i * CH, CH), CH)
-        value = cperm[rows, :]
-        value_b = value.astype(BF)
-        shift_here = sh[rows, :]
-        for d, (a_ref, b_ref) in enumerate(((af, bf), (ab, bb))):
-            decay_gate = jax.nn.sigmoid(dot(value_b, dgw[d, 0]))
-            input_gate = jax.nn.sigmoid(dot(value_b, igw[d, 0]))
-            log_decay = -8.0 * decay_gate * rate[d : d + 1, :] + shift_here
-            decay = jnp.exp(log_decay)
-            rest = one_minus_square(log_decay, decay)
-            root = rest * lax.rsqrt(jnp.maximum(rest, 1e-37))
-            a_ref[rows, :] = decay
-            b_ref[rows, :] = root * input_gate * value
-        return 0
-
-    lax.fori_loop(0, S // CH, gates, 0)
-
     def at(s):
         return pl.ds(pl.multiple_of(s * 8, 8), 8)
 
@@ -576,14 +572,16 @@
         lax.fori_loop(0, S // CH, finish, 0)
         stores[0].start()
 
-    near_arrived(0)
+    near_arrived(0, 0, G)
     for load in loads[10:13]:
         load.wait()
     for hop in range(1, H):
         for w in range(2):
             gather_hop(hop, w)
+        if hop == H - 2:
+            near_arrived(1, 0, G // 2)
         if hop == H - 1:
-            near_arrived(1)
+            near_arrived(1, G // 2 if H > 2 else 0, G)
         if hop > 1:
             reduce_step(2, hop - 2)
         for w in range(2):
@@ -647,8 +645,7 @@
     if G > 1:
         sent += [(near_send.at[0, pl.ds(0, GT - T)], near_ss.at[0])]
         sent += [(back.at[2, pl.ds(0, M - 2 * T)], ret_ss.at[2])]
-    for g in range(2):
-        mate_copy(g).wait_send()
+    sent += [(xn.at[g, c], mate_ss.at[g]) for g in range(2)]
     for block, sem in sent:
         pltpu.make_async_copy(block, block, sem).wait()
     for w in range(2):
@@ -668,6 +665,24 @@
         store.wait()
 
 
+def hand_over(rec_in, exp_in, rec_out, exp_out, rec, exp, in_sem, out_sem):
+    loads = [
+        pltpu.make_async_copy(rec_in, rec, in_sem.at[0]),
+        pltpu.make_async_copy(exp_in, exp, in_sem.at[1]),
+    ]
+    stores = [
+        pltpu.make_async_copy(rec, rec_out, out_sem.at[0]),
+        pltpu.make_async_copy(exp, exp_out, out_sem.at[1]),
+    ]
+    for load in loads:
+        load.start()
+    for load, store in zip(loads, stores):
+        load.wait()
+        store.start()
+    for store in stores:
+        store.wait()
+
+
 def local(
     E, T, x_path, gate_path, conv_taps, decay_gate_w, input_gate_w, decay_rate, decay_shift,
     expert_in, norm_gain, routes, route_scores, gate_weight, up_weight, down_weight,
@@ -675,7 +690,7 @@
     S = x_path.shape[0]
     R, D = expert_in.shape
     F = gate_weight.shape[2]
-    NY, H, K, HALF = T // 2, T // 4, E // 2, D // 2
+    NY, H, K, G, HALF = T // 2, T // 4, E // 2, E // 4, D // 2
     N, M = E * T, K * T
     hbm = pl.BlockSpec(memory_space=pltpu.HBM)
     dma = pltpu.SemaphoreType.DMA
@@ -738,7 +753,7 @@
         dma((2,)),
         dma((2,)),
         dma((2,)),
-        dma((2,)),
+        dma((2, G)),
         dma((2,)),
         dma((2,)),
         dma((2, 2, H)),
@@ -752,7 +767,7 @@
         dma((4,)),
         dma((2,)),
     ]
-    return pl.pallas_call(
+    results = pl.pallas_call(
         functools.partial(layer, E, T),
         out_shape=(
             jax.ShapeDtypeStruct((S, LANES), BF),
@@ -781,6 +796,15 @@
         routes.T,
         route_scores.T,
     )
+    return pl.pallas_call(
+        hand_over,
+        out_shape=tuple(jax.ShapeDtypeStruct(r.shape, r.dtype) for r in results),
+        in_specs=[hbm] * 2,
+        out_specs=(hbm, hbm),
+        scratch_shapes=[pltpu.VMEM(r.shape, r.dtype) for r in results] + [dma((2,)), dma((2,))],
+        compiler_params=pltpu.CompilerParams(vmem_limit_bytes=60 * 1024 * 1024),
+        name="hand_over",
+    )(*results)
 
 
 def solution(mesh):

time: 73.5 us -> 73.1 us (level)
  local copies, waits for them, and re-layouts: 2.33 us -> 0 us
  Pallas kernels: 69.4 us -> 71.2 us
    unnamed x4 -> x0, local copies, waits for them, and re-layouts: 2.33 us -> none
    pallas_call x0 -> x1, Pallas kernels: none -> 1.7 us  [local(): pl.pallas_call(hand_over, out_shape=tuple((jax.ShapeDtypeStruct(r.shape,...]
where the time goes in v5:
time: 73.1 us; the launch traced here: 71.9 us
  Pallas kernels  71.2 us (97%)
    pallas_call x1, Pallas kernels, local(): pl.pallas_call(functools.partial(layer, E, T), out_shape=(jax.ShapeDtypeS...  69.5 us
    pallas_call x1, Pallas kernels, local(): pl.pallas_call(hand_over, out_shape=tuple((jax.ShapeDtypeStruct(r.shape,...  1.7 us

profile of v5, /device:TPU:6, one launch (start us, length us, event | category | flops | bytes accessed | tf_op | source)
XLA Modules:
  0.0 71.9 jit_solution(4651975268099575276)
XLA Ops:
  0.6 69.5 %layer.1 = (bf16[1024,128]{1,0:T(8,128)(2,1)}, bf16[16,2048]{1,0:T(8,128)(2,1)}) custom-call(bf16[1024,128]{1,0:T(8,128)(2,1)} %x_hbm.1, bf16[1024,128]{1,0:T(8,128)(2,1)} %gate_hbm.1, bf16[256,2048]{1,0:T(8,128)(2,1)} %ein_hbm.1, bf16[2048,256]{1,0:T(8,128)(2,1)} %bitcast.7, bf16[2048,256]{1,0:T(8,128)(2,1)} %bitcast.8, bf16[256,2048]{1,0:T(8,128)(2,1)} %bitcast.9, ...), custom_call_target="tpu_custom_call" | custom-call | tf_op jit(solution)/shard_map/layer/pallas_call | solution.py:770
  70.2 1.7 %hand_over.1 = (bf16[1024,128]{1,0:T(8,128)(2,1)}, bf16[16,2048]{1,0:T(8,128)(2,1)}) custom-call(bf16[1024,128]{1,0:T(8,128)(2,1)} %get-tuple-element.4.rec_in, bf16[16,2048]{1,0:T(8,128)(2,1)} %get-tuple-element.5.exp_in), custom_call_target="tpu_custom_call" | custom-call | tf_op jit(solution)/shard_map/hand_over/pallas_call | solution.py:799

commit v6 on v5

--- a/solution.py
+++ b/solution.py
@@ -180,8 +180,8 @@
     greeted = list(range(K)) + list(range(E - 1, K - 1, -1))
 
     pairs = (
+        (ein_hbm, ein),
         (routes_hbm, routes_t),
-        (ein_hbm, ein),
         (gain_hbm, gain),
         (x_hbm, xraw),
         (taps_hbm, taps),
@@ -209,7 +209,7 @@
     for load in loads[4:]:
         load.start()
 
-    loads[0].wait()
+    loads[1].wait()
     ids = iota((E, R), 0)
     first_t = routes_t[0:1, :] == ids
     second_t = routes_t[1:2, :] == ids
@@ -228,7 +228,7 @@
     for w in range(2):
         for j in range(K):
             far_select[w, j * T : (j + 1) * T, :] = selector(w, K + j)
-    loads[1].wait()
+    loads[0].wait()
     loads[2].wait()
     total = jnp.zeros((R, LANES), F32)
     for j in range(D // LANES):
@@ -627,16 +627,6 @@
             table[w] = jnp.where(same_tile, wide, 0.0).astype(BF)
 
     second_pass()
-    arrivals = pl.ds(0, (E - 1) * T)
-    out = jnp.zeros((T * EXIT, LANES), F32)
-    for w in range(2):
-        block = ret_recv.at[w, arrivals]
-        pltpu.make_async_copy(block, block, ret_rs.at[w]).wait()
-        out = out + dot(c_hi[w], ret_recv[w]) + dot(c_lo[w], ret_recv[w])
-    for j in range(T):
-        exp_out[:, j * LANES : (j + 1) * LANES] = out[j * EXIT : (j + 1) * EXIT, :].astype(BF)
-    stores[1].start()
-
     tail.wait_send()
     head.wait_send()
     sent = [(carry_recv.at[pl.ds(0, E - 1)], carry_ss), (near_send.at[1], near_ss.at[1])]
@@ -661,6 +651,16 @@
                 for step in range(H):
                     if travels(direction, step, half):
                         sum_copy(v, direction, step, half).wait_send()
+    arrivals = pl.ds(0, (E - 1) * T)
+    out = jnp.zeros((T * EXIT, LANES), F32)
+    for w in range(2):
+        block = ret_recv.at[w, arrivals]
+        pltpu.make_async_copy(block, block, ret_rs.at[w]).wait()
+        out = out + dot(c_hi[w], ret_recv[w]) + dot(c_lo[w], ret_recv[w])
+    for j in range(T):
+        exp_out[:, j * LANES : (j + 1) * LANES] = out[j * EXIT : (j + 1) * EXIT, :].astype(BF)
+    stores[1].start()
+
     for store in stores:
         store.wait()
 

time: 73.1 us -> 73.7 us (level)
  the two profiles are of different devices: /device:TPU:6 before, /device:TPU:1 now
where the time goes in v6:
time: 73.7 us; the launch traced here: 73.6 us
  Pallas kernels  72.9 us (99%)
    pallas_call x1, Pallas kernels, local(): pl.pallas_call(functools.partial(layer, E, T), out_shape=(jax.ShapeDtypeS...  71.2 us
    pallas_call x1, Pallas kernels, local(): pl.pallas_call(hand_over, out_shape=tuple((jax.ShapeDtypeStruct(r.shape,...  1.7 us

profile of v6, /device:TPU:1, one launch (start us, length us, event | category | flops | bytes accessed | tf_op | source)
XLA Modules:
  0.0 73.6 jit_solution(7577903320088421216)
XLA Ops:
  0.6 71.2 %layer.1 = (bf16[1024,128]{1,0:T(8,128)(2,1)}, bf16[16,2048]{1,0:T(8,128)(2,1)}) custom-call(bf16[1024,128]{1,0:T(8,128)(2,1)} %x_hbm.1, bf16[1024,128]{1,0:T(8,128)(2,1)} %gate_hbm.1, bf16[256,2048]{1,0:T(8,128)(2,1)} %ein_hbm.1, bf16[2048,256]{1,0:T(8,128)(2,1)} %bitcast.7, bf16[2048,256]{1,0:T(8,128)(2,1)} %bitcast.8, bf16[256,2048]{1,0:T(8,128)(2,1)} %bitcast.9, ...), custom_call_target="tpu_custom_call" | custom-call | tf_op jit(solution)/shard_map/layer/pallas_call | solution.py:770
  71.9 1.7 %hand_over.1 = (bf16[1024,128]{1,0:T(8,128)(2,1)}, bf16[16,2048]{1,0:T(8,128)(2,1)}) custom-call(bf16[1024,128]{1,0:T(8,128)(2,1)} %get-tuple-element.4.rec_in, bf16[16,2048]{1,0:T(8,128)(2,1)} %get-tuple-element.5.exp_in), custom_call_target="tpu_custom_call" | custom-call | tf_op jit(solution)/shard_map/hand_over/pallas_call | solution.py:799
